TPU v7x, 32 devices: a whole 2x2x4 slice. The times are simulated.
32 devices in a mesh: ep: 8 (over z, y), tp: 4 (over x, core).
Axes of the slice: x: 2, y: 2, z: 4, core: 2. Of those that a mesh axis runs over, the one named last changes fastest.
Arguments:
- tokens: bfloat16 [64, 2048], P('ep'), may hold values from -4 to 4
- w_query: bfloat16 [2048, 1024], P(None, 'tp'), may hold values from -0.125 to 0.125
- w_key: bfloat16 [2048, 1024], P(None, 'tp'), may hold values from -0.125 to 0.125
- w_value: bfloat16 [2048, 1024], P(None, 'tp'), may hold values from -0.125 to 0.125
- w_outgate: bfloat16 [2048, 1024], P(None, 'tp'), may hold values from -0.125 to 0.125
- w_igate: bfloat16 [2048, 4], P(None, 'tp'), may hold values from -0.125 to 0.125
- w_fgate: bfloat16 [2048, 4], P(None, 'tp'), may hold values from -0.125 to 0.125
- forget_bias: float32 [4], P('tp'), may hold values from -1 to 5
- w_out: bfloat16 [1024, 2048], P('tp'), may hold values from -0.1875 to 0.1875
- gain_mix: float32 [2048], replicated, may hold values from 0.1 to 1.9
- gain_moe: float32 [2048], replicated, may hold values from 0.1 to 1.9
- memory: float32 [64, 4, 256, 256], P('ep', 'tp'), may hold values from -0.4 to 0.4
- normalizer: float32 [64, 4, 256], P('ep', 'tp'), may hold values from -0.8 to 0.8
- stabilizer: float32 [64, 4], P('ep', 'tp'), may hold values from 0 to 2
- expert_gate: bfloat16 [8, 2048, 512], P('ep', None, 'tp'), may hold values from -0.125 to 0.125
- expert_up: bfloat16 [8, 2048, 512], P('ep', None, 'tp'), may hold values from -0.125 to 0.125
- expert_down: bfloat16 [8, 512, 2048], P('ep', 'tp'), may hold values from -1 to 1
- routes: int32 [64, 4], P('ep'), may hold values from 0 to 7, all different within a row; in each aligned block of 8 rows (0 to 7, 8 to 15, ...) at most 8 rows name the same one
- route_weight: float32 [64, 4], P('ep'), may hold values from 0.2 to 1
Outputs:
- output: bfloat16 [64, 2048], P('ep', 'tp')
- memory_next: float32 [64, 4, 256, 256], P('ep', 'tp')
- norm_next: float32 [64, 4, 256], P('ep', 'tp')
- stabilizer_next: float32 [64, 4], P('ep', 'tp')
Inputs may be any that keep to these rules, and one draw needn't show every extreme that they name: `routes`: each row names 4 different experts. Among the 8 rows of one device (aligned blocks), no expert is named more than 8 times, a bound that some block reaches.
All inputs are finite; a program needn't handle non-finite values.
Results may differ from a plain program's by a relative error of at most 0.029.
Values may be sent and summed in bfloat16 or wider, within the bound.
No kernel may reach another device: no remote copies, remote signals or barrier semaphores. Data moves between devices by JAX's collectives and lax.ppermute only.
A program may use at most 64 MiB of HBM per device.

v0:
```python
import math

import jax
import jax.numpy as jnp
from jax import lax
from jax.sharding import PartitionSpec as P


def layer_norm(row_data, gain_vec):
    values = row_data.astype(jnp.float32)
    row_mean = jnp.mean(values, -1, keepdims=True)
    centered = values - row_mean
    variance = jnp.mean(centered * centered, -1, keepdims=True)
    return centered * lax.rsqrt(variance + 1e-05) * gain_vec


def slot_targets(routes, experts, capacity):
    flat_routes = routes.reshape(-1)
    onehot = (flat_routes[:, None] == jnp.arange(experts, dtype=jnp.int32)[None, :]).astype(
        jnp.int32
    )
    before = jnp.cumsum(onehot, axis=0) - onehot
    slot_index = jnp.sum(before * onehot, axis=1)
    return flat_routes * capacity + slot_index


def shards(
    tokens,
    w_query,
    w_key,
    w_value,
    w_outgate,
    w_igate,
    w_fgate,
    forget_bias,
    w_out,
    gain_mix,
    gain_moe,
    memory,
    normalizer,
    stabilizer,
    expert_gate,
    expert_up,
    expert_down,
    routes,
    route_weight,
):
    seq_rows = tokens.shape[0]
    model_width = tokens.shape[1]
    head_count = memory.shape[1]
    head_size = memory.shape[2]
    head_cols = head_count * head_size
    normed = layer_norm(tokens, gain_mix).astype(jnp.bfloat16)
    gate_in = jnp.dot(normed, w_igate, preferred_element_type=jnp.float32)
    gate_forget = jnp.dot(normed, w_fgate, preferred_element_type=jnp.float32)
    weights = (w_query, w_key, w_value, w_outgate)
    projected = jnp.concatenate(
        [jnp.dot(normed, weight, preferred_element_type=jnp.float32) for weight in weights], axis=1
    )
    rounded = projected.astype(jnp.bfloat16).reshape(seq_rows, 4, head_count, head_size)
    queries = rounded[:, 0].astype(jnp.float32)
    keys_scaled = rounded[:, 1].astype(jnp.float32) / math.sqrt(head_size)
    values_rows = rounded[:, 2].astype(jnp.float32)
    out_gate = rounded[:, 3].astype(jnp.float32)
    log_forget = jax.nn.log_sigmoid(gate_forget + forget_bias)
    stabilizer_next = jnp.maximum(log_forget + stabilizer, gate_in)
    keep_rate = jnp.exp(log_forget + stabilizer - stabilizer_next)
    admit_rate = jnp.exp(gate_in - stabilizer_next)
    memory_next = (
        keep_rate[:, :, None, None] * memory
        + admit_rate[:, :, None, None] * keys_scaled[:, :, :, None] * values_rows[:, :, None, :]
    )
    norm_next = keep_rate[:, :, None] * normalizer + admit_rate[:, :, None] * keys_scaled
    numerator = jnp.einsum("shk,shkv->shv", queries, memory_next, precision=lax.Precision.HIGHEST)
    denominator = jnp.sum(queries * norm_next, axis=-1)
    readout = numerator / jnp.maximum(jnp.abs(denominator), jnp.exp(-stabilizer_next))[:, :, None]
    mixed = (jax.nn.sigmoid(out_gate) * readout).astype(jnp.bfloat16).reshape(seq_rows, head_cols)
    head_part = jnp.dot(mixed, w_out, preferred_element_type=jnp.float32).astype(jnp.bfloat16)
    summed = lax.psum(head_part, "tp").astype(jnp.float32)
    residual = tokens.astype(jnp.float32) + summed
    expert_in = layer_norm(residual, gain_moe).astype(jnp.bfloat16)
    top_count = routes.shape[1]
    local_experts = expert_gate.shape[0]
    expert_count = local_experts * lax.axis_size("ep")
    capacity = max(2, 2 * seq_rows * top_count // expert_count)
    target = slot_targets(routes, expert_count, capacity)
    outbound = (
        jnp.zeros((expert_count * capacity, model_width), jnp.bfloat16)
        .at[target]
        .set(jnp.repeat(expert_in, top_count, axis=0))
    )
    outbound = outbound.reshape(expert_count, capacity, model_width)
    quarter = model_width // lax.axis_size("tp")
    arrived = lax.all_to_all(outbound, "ep", split_axis=0, concat_axis=0, tiled=True)
    slot_count = arrived.shape[1]
    grouped = arrived.reshape(-1, local_experts, slot_count, model_width)
    gate_part = jnp.einsum(
        "aecd,edf->aecf", grouped, expert_gate, preferred_element_type=jnp.float32
    )
    up_part = jnp.einsum("aecd,edf->aecf", grouped, expert_up, preferred_element_type=jnp.float32)
    hidden = (jax.nn.silu(gate_part) * up_part).astype(jnp.bfloat16)
    partial_value, slot_count = (
        jnp.einsum("aecf,efd->aecd", hidden, expert_down, preferred_element_type=jnp.float32),
        slot_count,
    )
    reduced = lax.psum_scatter(partial_value, "tp", scatter_dimension=3, tiled=True).astype(
        jnp.bfloat16
    )
    reduced = reduced.reshape(-1, slot_count, reduced.shape[3])
    returned = lax.all_to_all(reduced, "ep", split_axis=0, concat_axis=0, tiled=True)
    picked = jnp.take(returned.reshape(expert_count * capacity, quarter), target, axis=0).reshape(
        seq_rows, top_count, quarter
    )
    combined = jnp.sum(route_weight[:, :, None] * picked.astype(jnp.float32), axis=1)
    own_cols = lax.dynamic_slice_in_dim(residual, lax.axis_index("tp") * quarter, quarter, 1)
    output = (own_cols + combined).astype(jnp.bfloat16)
    return (output, memory_next, norm_next, stabilizer_next)


def solution(mesh):
    return jax.shard_map(
        shards,
        mesh=mesh,
        in_specs=(
            P("ep", None),
            P(None, "tp"),
            P(None, "tp"),
            P(None, "tp"),
            P(None, "tp"),
            P(None, "tp"),
            P(None, "tp"),
            P("tp"),
            P("tp", None),
            P(),
            P(),
            P("ep", "tp", None, None),
            P("ep", "tp", None),
            P("ep", "tp"),
            P("ep", None, "tp"),
            P("ep", None, "tp"),
            P("ep", "tp", None),
            P("ep", None),
            P("ep", None),
        ),
        out_specs=(P("ep", "tp"), P("ep", "tp", None, None), P("ep", "tp", None), P("ep", "tp")),
        check_vma=False,
    )
```

profile of v0, /device:TPU:0, one launch (start us, length us, event | category | flops | bytes accessed | tf_op | source)
XLA Modules:
  0.0 94.1 jit_solution(10027938302184542748)
XLA Ops:
  7.2 0.9 copy.30
  8.1 0.1 reshape.339
  8.2 1.0 %convert_reduce_fusion = f32[8]{0:T(128)S(1)} fusion(bf16[8,2048]{1,0:T(8,128)(2,1)} %param.19), kind=kLoop, calls=%fused_computation.36 | loop fusion | flops 32760 | bytes 32800 | tf_op jit(solution)/shard_map/reduce_sum | solution.py:11
  9.3 1.0 %fusion.24 = f32[8]{0:T(128)S(1)} fusion(bf16[8,2048]{1,0:T(8,128)(2,1)} %param.19, f32[8]{0:T(128)S(1)} %broadcast_multiply_fusion.3), kind=kLoop, calls=%fused_computation.39 | loop fusion | flops 65528 | bytes 32832 | tf_op jit(solution)/shard_map/reduce_sum | solution.py:13
  10.9 0.8 fusion.26
  11.7 0.8 convolution_bitcast_fusion.3
  12.6 0.8 exponential_bitcast_fusion
  13.4 1.5 %fusion.5 = f32[8,256]{1,0:T(8,128)S(1)} fusion(bf16[8,2048]{1,0:T(8,128)(2,1)S(1)} %fusion.26, bf16[2048,256]{1,0:T(8,128)(2,1)} %param.22), kind=kOutput, calls=%fused_computation.13 | convolution fusion | flops 8392704 | bytes 1089536 | tf_op jit(solution)/shard_map/dot_general | solution.py:58
  14.9 1.4 %broadcast_multiply_fusion = (f32[8,256]{1,0:T(8,128)S(1)}, f32[8,256]{1,0:T(8,128)S(1)}) fusion(f32[8]{0:T(128)S(1)} %multiply_bitcast_fusion, bf16[8,2048]{1,0:T(8,128)(2,1)S(1)} %fusion.26, bf16[2048,256]{1,0:T(8,128)(2,1)} %param.21), kind=kOutput, calls=%fused_computation.68 | convolution fusion | flops 8394752 | bytes 1097760 | tf_op jit(solution)/shard_map/dot_general | solution.py:58
  16.4 0.4 fusion.34
  16.8 0.5 multiply_add_fusion
  17.3 0.8 fusion
  18.1 2.0 %convolution_convert_fusion = bf16[8,2048]{1,0:T(8,128)(2,1)S(1)} fusion(bf16[256,2048]{1,0:T(8,128)(2,1)S(1)} %copy-done, bf16[8,2048]{1,0:T(8,128)(2,1)S(1)} %fusion.26, bf16[2048,256]{1,0:T(8,128)(2,1)} %param.23, f32[8,1,256]{2,1,0:T(1,128)S(1)} %fusion, f32[8]{0:T(128)S(1)} %fusion.42), kind=kOutput, calls=%fused_computation.3 | convolution fusion | flops 16809984 | bytes 2170912 | tf_op jit(solution)/shard_map/dot_general | solution.py:78
  20.1 12.9 %psum.7 = bf16[8,2048]{1,0:T(8,128)(2,1)S(1)} all-reduce(bf16[8,2048]{1,0:T(8,128)(2,1)S(1)} %convolution_convert_fusion), channel_id=1, replica_groups=mesh['ep'=8,'tp'=4] {'tp'}, use_global_device_ids=true, to_apply=%region_3.4 | all-reduce | flops 16384 | bytes 65536 | tf_op jit(solution)/shard_map/psum | solution.py:79
  33.0 0.1 convert_add_fusion
  33.2 0.2 multiply_reduce_fusion.1
  33.4 0.1 multiply_convert_fusion
  33.7 0.2 select_reduce_fusion
  33.9 0.1 mul.192
  34.0 0.9 scatter_custom_fusion
  34.9 13.9 %all_to_all.10 = bf16[8,8,2048]{2,1,0:T(8,128)(2,1)S(1)} all-to-all(bf16[8,8,2048]{2,1,0:T(8,128)(2,1)S(1)} %bitcast.115), channel_id=1, replica_groups=mesh['ep'=8,'tp'=4] {'ep'}, dimensions={0} | all-to-all | bytes 524288 | tf_op jit(solution)/shard_map/all_to_all | solution.py:94
  48.7 1.3 %convolution_bitcast_fusion.2 = f32[8,1,8,128]{3,2,0,1:T(8,128)S(1)} fusion(bf16[8,8,2048]{2,1,0:T(8,128)(2,1)S(1)} %all_to_all.10, bf16[1,2048,128]{2,1,0:T(8,128)(2,1)} %param.33), kind=kOutput, calls=%fused_computation.9 | convolution fusion | flops 33554432 | bytes 819200 | tf_op jit(solution)/shard_map/aecd,edf->aecf/dot_general | solution.py:97
  50.0 1.2 %convolution_bitcast_fusion = f32[8,1,8,2048]{3,2,0,1:T(8,128)} fusion(bf16[8,8,2048]{2,1,0:T(8,128)(2,1)S(1)} %all_to_all.10, bf16[1,128,2048]{2,1,0:T(8,128)(2,1)S(1)} %copy-done.5, bf16[1,2048,128]{2,1,0:T(8,128)(2,1)S(1)} %copy-done.6, f32[8,1,8,128]{3,2,0,1:T(8,128)S(1)} %convolution_bitcast_fusion.2), kind=kOutput, calls=%fused_computation.2 | convolution fusion | flops 67158016 | bytes 1867776 | tf_op jit(solution)/shard_map/aecf,efd->aecd/dot_general | solution.py:103
  51.3 20.7 %reduce-scatter.2.cloned.1.call-done = f32[8,1,8,512]{3,2,0,1:T(8,128)} async-done(((f32[8,1,8,2048]{3,2,0,1:T(8,128)}), f32[8,1,8,512]{3,2,0,1:T(8,128)}) %reduce-scatter.2.cloned.1.call-update) | async-done | bytes 131088 | tf_op jit(solution)/shard_map/reduce_scatter | solution.py:106
  72.0 1.5 %convert_bitcast_fusion = bf16[8,8,512]{2,1,0:T(8,128)(2,1)} fusion(f32[8,1,8,512]{3,2,0,1:T(8,128)} %reduce-scatter.2.cloned.1.call-done), kind=kLoop, calls=%fused_computation.43 | loop fusion | flops 32768 | bytes 196608 | tf_op jit(solution)/shard_map/reshape | solution.py:109
  73.5 5.5 %all-to-all-start.1 = ((bf16[8,8,512]{2,1,0:T(8,128)(2,1)}), bf16[8,8,512]{2,1,0:T(8,128)(2,1)S(1)}, u32[]{:S(2)}, u32[]{:S(2)}) async-start(bf16[8,8,512]{2,1,0:T(8,128)(2,1)} %convert_bitcast_fusion), calls=%async_computation.2 | async-start | bytes 131072 | tf_op jit(solution)/shard_map/all_to_all | solution.py:110
  79.0 0.1 copy.29
  79.1 0.6 copy.32
  79.7 6.2 %all-to-all-done.1 = bf16[8,8,512]{2,1,0:T(8,128)(2,1)S(1)} async-done(((bf16[8,8,512]{2,1,0:T(8,128)(2,1)}), bf16[8,8,512]{2,1,0:T(8,128)(2,1)S(1)}, u32[]{:S(2)}, u32[]{:S(2)}) %all-to-all-start.1) | async-done | bytes 65568 | tf_op jit(solution)/shard_map/all_to_all | solution.py:110
  85.9 0.6 gather_fusion
  86.6 0.1 multiply_reduce_fusion
  86.7 0.6 add_convert_fusion
  (40 shorter events, 0.5 us)
Async XLA Ops:
  7.2 11.0 %copy-start = (bf16[256,2048]{1,0:T(8,128)(2,1)S(1)}, bf16[256,2048]{1,0:T(8,128)(2,1)}, u32[]{:S(2)}) copy-start(bf16[256,2048]{1,0:T(8,128)(2,1)} %param.27) | copy-start | bytes 3145732
  7.2 9.2 %copy-start.4 = (bf16[2048,256]{1,0:T(8,128)(2,1)S(1)}, bf16[2048,256]{1,0:T(8,128)(2,1)}, u32[]{:S(2)}) copy-start(bf16[2048,256]{1,0:T(8,128)(2,1)} %param.20) | copy-start | bytes 3145732
  7.2 9.2 %copy-start.7 = (f32[8,1,256]{2,1,0:T(1,128)S(1)}, f32[8,1,256]{2,1,0:T(1,128)}, u32[]{:S(2)}) copy-start(f32[8,1,256]{2,1,0:T(1,128)} %param.31) | copy-start | bytes 24580
  7.2 64.8 %reduce-scatter.2.cloned.1.call-start = ((), (), s32[]{:S(2)}) async-start(), calls=%async_computation.3 | async-start | bytes 655360 | tf_op jit(solution)/shard_map/reduce_scatter | solution.py:106
  8.2 8.6 %copy-start.2 = (f32[8,1,256,256]{3,2,1,0:T(8,128)S(1)}, f32[8,1,256,256]{3,2,1,0:T(8,128)}, u32[]{:S(2)}) copy-start(f32[8,1,256,256]{3,2,1,0:T(8,128)} %param.30) | copy-start | bytes 6291460
  13.4 3.8 %copy-start.10 = (f32[8,1]{0,1:T(1,128)}, f32[8,1]{0,1:T(1,128)S(1)}, u32[]{:S(2)}) copy-start(f32[8,1]{0,1:T(1,128)S(1)} %get-tuple-element.15) | copy-start | bytes 100
  17.3 2.8 %copy-start.1 = (f32[8,1,256,256]{3,2,1,0:T(8,128)}, f32[8,1,256,256]{3,2,1,0:T(8,128)S(1)}, u32[]{:S(2)}) copy-start(f32[8,1,256,256]{3,2,1,0:T(8,128)S(1)} %multiply_add_fusion) | copy-start | bytes 6291460
  17.3 15.7 %copy-start.3 = (bf16[8,2048]{1,0:T(8,128)(2,1)S(1)}, bf16[8,2048]{1,0:T(8,128)(2,1)}, u32[]{:S(2)}) copy-start(bf16[8,2048]{1,0:T(8,128)(2,1)} %param.19) | copy-start | bytes 98308
  17.3 16.1 %copy-start.8 = (f32[2048]{0:T(1024)S(1)}, f32[2048]{0:T(1024)}, u32[]{:S(2)}) copy-start(f32[2048]{0:T(1024)} %param.29) | copy-start | bytes 24580
  33.0 17.0 %copy-start.5 = (bf16[1,128,2048]{2,1,0:T(8,128)(2,1)S(1)}, bf16[1,128,2048]{2,1,0:T(8,128)(2,1)}, u32[]{:S(2)}) copy-start(bf16[1,128,2048]{2,1,0:T(8,128)(2,1)} %param.35) | copy-start | bytes 1572868
  33.0 17.0 %copy-start.6 = (bf16[1,2048,128]{2,1,0:T(8,128)(2,1)S(1)}, bf16[1,2048,128]{2,1,0:T(8,128)(2,1)}, u32[]{:S(2)}) copy-start(bf16[1,2048,128]{2,1,0:T(8,128)(2,1)} %param.34) | copy-start | bytes 1572868
  34.9 44.2 %copy-start.9 = (f32[8,4]{0,1:T(4,128)S(1)}, f32[8,4]{0,1:T(4,128)}, u32[]{:S(2)}) copy-start(f32[8,4]{0,1:T(4,128)} %param.37) | copy-start | bytes 388
  73.5 12.4 %all-to-all-start.1 = ((bf16[8,8,512]{2,1,0:T(8,128)(2,1)}), bf16[8,8,512]{2,1,0:T(8,128)(2,1)S(1)}, u32[]{:S(2)}, u32[]{:S(2)}) async-start(bf16[8,8,512]{2,1,0:T(8,128)(2,1)} %convert_bitcast_fusion), calls=%async_computation.2 | async-start | bytes 131072 | tf_op jit(solution)/shard_map/all_to_all | solution.py:110
Sparse Core Ops, SparseCore 0:
  51.3 20.5 reduce-scatter.1
where the time goes:
time: 94.8 us; the launch traced here: 94.1 us
  waiting for transfers between devices  26.9 us (28%)
  blocking collectives  26.8 us (28%)
  between operations  14.9 us (16%)
  matrix products  10.2 us (11%)
  other arithmetic  6.35 us (7%)
  starting transfers between devices  5.55 us (6%)
  local copies, waits for them, and re-layouts  3.52 us (4%)
    reduce_scatter x1, waiting for transfers between devices, shards(): lax.psum_scatter(partial_value, 'tp', scatter_dimension=3, tiled=True)  20.7 us
    all_to_all x1, blocking collectives, shards(): lax.all_to_all(outbound, 'ep', split_axis=0, concat_axis=0, tiled=True)  13.9 us
    psum x1, blocking collectives, shards(): summed = lax.psum(head_part, 'tp').astype(jnp.float32)  12.9 us
    all_to_all x1, waiting for transfers between devices, shards(): lax.all_to_all(reduced, 'ep', split_axis=0, concat_axis=0, tiled=True)  6.19 us
    all_to_all x1, starting transfers between devices, shards(): lax.all_to_all(reduced, 'ep', split_axis=0, concat_axis=0, tiled=True)  5.52 us
    dot_general x3, matrix products, shards(): jnp.dot(normed, weight, preferred_element_type=jnp.float32)  3.27 us
    dot_general x1, matrix products, shards(): jnp.dot(mixed, w_out, preferred_element_type=jnp.float32)  1.96 us
  transfers between devices with their start and end apart: 2, of which 2 were waited for; matrix products, arithmetic and copies ran while one was open for 1% of the time, Pallas kernels for 0%

commit v1 on v0

v1 whole, which is shorter than its diff:
```python
import math

import jax
import jax.numpy as jnp
from jax import lax
from jax.sharding import PartitionSpec as P

BOTH = ("ep", "tp")


def layer_norm(row_data, gain_vec):
    values = row_data.astype(jnp.float32)
    row_mean = jnp.mean(values, -1, keepdims=True)
    centered = values - row_mean
    variance = jnp.mean(centered * centered, -1, keepdims=True)
    return centered * lax.rsqrt(variance + 1e-05) * gain_vec


def shards(
    tokens,
    w_query,
    w_key,
    w_value,
    w_outgate,
    w_igate,
    w_fgate,
    forget_bias,
    w_out,
    gain_mix,
    gain_moe,
    memory,
    normalizer,
    stabilizer,
    expert_gate,
    expert_up,
    expert_down,
    routes,
    route_weight,
):
    ep_size = lax.axis_size("ep")
    tp_size = lax.axis_size("tp")
    seq_rows, model_width = tokens.shape
    head_count = memory.shape[1]
    head_size = memory.shape[2]
    head_cols = head_count * head_size
    quarter = model_width // tp_size
    half = seq_rows // 2
    duo = tp_size // 2
    ep_id = lax.axis_index("ep")
    tp_id = lax.axis_index("tp")
    side = tp_id % 2
    swap = [(t, t ^ 1) for t in range(tp_size)]
    same_side = [
        [e * tp_size + x * 2 + c for e in range(ep_size) for x in range(duo)] for c in range(2)
    ]
    mate_gate = lax.ppermute(expert_gate[0], "tp", swap)
    mate_up = lax.ppermute(expert_up[0], "tp", swap)
    mate_down = lax.ppermute(expert_down[0], "tp", swap)

    normed = layer_norm(tokens, gain_mix).astype(jnp.bfloat16)
    gate_in = jnp.dot(normed, w_igate, preferred_element_type=jnp.float32)
    gate_forget = jnp.dot(normed, w_fgate, preferred_element_type=jnp.float32)
    queries, keys, values_rows, out_gate = [
        jnp.dot(normed, weight, preferred_element_type=jnp.float32)
        .astype(jnp.bfloat16)
        .astype(jnp.float32)
        .reshape(seq_rows, head_count, head_size)
        for weight in (w_query, w_key, w_value, w_outgate)
    ]
    keys_scaled = keys / math.sqrt(head_size)
    log_forget = jax.nn.log_sigmoid(gate_forget + forget_bias)
    stabilizer_next = jnp.maximum(log_forget + stabilizer, gate_in)
    keep_rate = jnp.exp(log_forget + stabilizer - stabilizer_next)
    admit_rate = jnp.exp(gate_in - stabilizer_next)
    memory_next = (
        keep_rate[:, :, None, None] * memory
        + admit_rate[:, :, None, None] * keys_scaled[:, :, :, None] * values_rows[:, :, None, :]
    )
    norm_next = keep_rate[:, :, None] * normalizer + admit_rate[:, :, None] * keys_scaled
    numerator = jnp.einsum("shk,shkv->shv", queries, memory_next, precision=lax.Precision.HIGHEST)
    denominator = jnp.sum(queries * norm_next, axis=-1)
    readout = numerator / jnp.maximum(jnp.abs(denominator), jnp.exp(-stabilizer_next))[:, :, None]
    mixed = (jax.nn.sigmoid(out_gate) * readout).astype(jnp.bfloat16).reshape(seq_rows, head_cols)
    head_part = jnp.dot(mixed, w_out, preferred_element_type=jnp.float32)
    own_token = jnp.where(tp_id < 2, 1.0, 0.0) * tokens.astype(jnp.float32)

    first = side == 0
    sent = jnp.where(first, head_part[half:], head_part[:half]).astype(jnp.bfloat16)
    kept = head_part + own_token
    kept = jnp.where(first, kept[:half], kept[half:])
    met = lax.ppermute(sent, "tp", swap)
    pair_sum = (kept + met.astype(jnp.float32)).astype(jnp.bfloat16)
    outbound = jnp.broadcast_to(pair_sum[None], (ep_size * duo, half, model_width))
    arrived = lax.all_to_all(
        outbound, BOTH, 0, 0, tiled=True, axis_index_groups=same_side
    )
    residual = jnp.sum(
        arrived.reshape(ep_size, duo, half, model_width).astype(jnp.float32), axis=1
    )
    own_rows = lax.dynamic_index_in_dim(residual, ep_id, 0, keepdims=False)
    for_mate = lax.dynamic_slice_in_dim(own_rows, (tp_id ^ 1) * quarter, quarter, 1)
    for_self = lax.dynamic_slice_in_dim(own_rows, tp_id * quarter, quarter, 1)
    from_mate = lax.ppermute(for_mate, "tp", swap)

    expert_in = layer_norm(residual.reshape(-1, model_width), gain_moe).astype(jnp.bfloat16)

    def one(gate_w, up_w, down_w):
        gate_part = jnp.dot(expert_in, gate_w, preferred_element_type=jnp.float32)
        up_part = jnp.dot(expert_in, up_w, preferred_element_type=jnp.float32)
        hidden = (jax.nn.silu(gate_part) * up_part).astype(jnp.bfloat16)
        return jnp.dot(hidden, down_w, preferred_element_type=jnp.float32)

    part = one(expert_gate[0], expert_up[0], expert_down[0]) + one(mate_gate, mate_up, mate_down)
    blocks = (
        part.astype(jnp.bfloat16)
        .reshape(ep_size, half, tp_size, quarter)
        .transpose(0, 2, 1, 3)
        .reshape(ep_size * tp_size, half, quarter)
    )
    returned = lax.all_to_all(blocks, BOTH, 0, 0, tiled=True)
    per_expert = jnp.sum(
        returned.reshape(ep_size, duo, 2, half, quarter).astype(jnp.float32), axis=1
    )
    share = jnp.sum(
        jnp.where(
            routes[:, :, None] == jnp.arange(ep_size, dtype=jnp.int32)[None, None, :],
            route_weight[:, :, None],
            0.0,
        ),
        axis=1,
    )
    combined = jnp.sum(
        share.T[:, :, None] * per_expert.reshape(ep_size, seq_rows, quarter), axis=0
    )
    own_cols = jnp.concatenate(
        [jnp.where(first, for_self, from_mate), jnp.where(first, from_mate, for_self)], axis=0
    )
    output = (own_cols + combined).astype(jnp.bfloat16)
    return (output, memory_next, norm_next, stabilizer_next)


def solution(mesh):
    return jax.shard_map(
        shards,
        mesh=mesh,
        in_specs=(
            P("ep", None),
            P(None, "tp"),
            P(None, "tp"),
            P(None, "tp"),
            P(None, "tp"),
            P(None, "tp"),
            P(None, "tp"),
            P("tp"),
            P("tp", None),
            P(),
            P(),
            P("ep", "tp", None, None),
            P("ep", "tp", None),
            P("ep", "tp"),
            P("ep", None, "tp"),
            P("ep", None, "tp"),
            P("ep", "tp", None),
            P("ep", None),
            P("ep", None),
        ),
        out_specs=(P("ep", "tp"), P("ep", "tp", None, None), P("ep", "tp", None), P("ep", "tp")),
        check_vma=False,
    )
```

time: 94.8 us -> 57.2 us (0.60)
  blocking collectives: 26.8 us -> 0 us
  between operations: 14.9 us -> 1.63 us
  waiting for transfers between devices: 26.9 us -> 17.8 us
  starting transfers between devices: 5.55 us -> 12 us
  matrix products: 10.2 us -> 12.5 us
  local copies, waits for them, and re-layouts: 3.52 us -> 5.34 us
    reduce_scatter x1 -> x0, waiting for transfers between devices: 20.7 us -> none  [shards(): lax.psum_scatter(partial_value, 'tp', scatter_dimension=3, tiled=True)]
    all_to_all x1 -> x0, blocking collectives: 13.9 us -> none  [shards(): lax.all_to_all(outbound, 'ep', split_axis=0, concat_axis=0, tiled=True)]
    psum x1 -> x0, blocking collectives: 12.9 us -> none  [shards(): summed = lax.psum(head_part, 'tp').astype(jnp.float32)]
    all_to_all x1 -> x2, waiting for transfers between devices: 6.19 us -> 16.9 us  [the longest x1 9.54 us: shards(): lax.all_to_all(outbound, BOTH, 0, 0, tiled=True, axis_index_groups=same_s...]
    all_to_all x1 -> x2, starting transfers between devices: 5.52 us -> 10.8 us  [the longest x1 8.19 us: shards(): lax.all_to_all(outbound, BOTH, 0, 0, tiled=True, axis_index_groups=same_s...]
    dot_general x3 -> x5, matrix products: 4.4 us -> 6.71 us  [the longest x2 2.66 us: one(): return jnp.dot(hidden, down_w, preferred_element_type=jnp.float32)]
    reshape x1 -> x0, other arithmetic: 1.53 us -> none  [shards(): reduced = reduced.reshape(-1, slot_count, reduced.shape[3])]
    add x1, other arithmetic: 0.47 us -> 1.95 us  [shards(): keep_rate[:, :, None, None] * memory]
  transfers between devices with their start and end apart: 2 -> 7, of which waited for: 2 -> 3; matrix products, arithmetic and copies ran while one was open for 1% -> 19% of each run, Pallas kernels for 0% -> 0%
where the time goes in v1:
time: 57.2 us; the launch traced here: 56.4 us
  waiting for transfers between devices  17.8 us (31%)
  matrix products  12.5 us (22%)
  starting transfers between devices  12 us (21%)
  other arithmetic  7.17 us (13%)
  local copies, waits for them, and re-layouts  5.34 us (9%)
  between operations  1.63 us (3%)
    all_to_all x1, waiting for transfers between devices, shards(): lax.all_to_all(outbound, BOTH, 0, 0, tiled=True, axis_index_groups=same_s...  9.54 us
    all_to_all x1, starting transfers between devices, shards(): lax.all_to_all(outbound, BOTH, 0, 0, tiled=True, axis_index_groups=same_s...  8.19 us
    all_to_all x1, waiting for transfers between devices, shards(): returned = lax.all_to_all(blocks, BOTH, 0, 0, tiled=True)  7.38 us
    dot_general x3, matrix products, shards(): jnp.dot(normed, weight, preferred_element_type=jnp.float32)  3.27 us
    dot_general x2, matrix products, one(): return jnp.dot(hidden, down_w, preferred_element_type=jnp.float32)  2.66 us
    all_to_all x1, starting transfers between devices, shards(): returned = lax.all_to_all(blocks, BOTH, 0, 0, tiled=True)  2.62 us
    dot_general x1, matrix products, shards(): head_part = jnp.dot(mixed, w_out, preferred_element_type=jnp.float32)  1.97 us
    add x1, other arithmetic, shards(): keep_rate[:, :, None, None] * memory  1.95 us
  transfers between devices with their start and end apart: 7, of which 3 were waited for; matrix products, arithmetic and copies ran while one was open for 19% of the time, Pallas kernels for 0%

profile of v1, /device:TPU:0, one launch (start us, length us, event | category | flops | bytes accessed | tf_op | source)
XLA Modules:
  0.0 56.4 jit_solution(5236270454450020484)
XLA Ops:
  0.7 1.0 %convert_reduce_fusion.2 = f32[8]{0:T(128)S(1)} fusion(bf16[8,2048]{1,0:T(8,128)(2,1)} %param.19), kind=kLoop, calls=%fused_computation.36 | loop fusion | flops 32760 | bytes 32800 | tf_op jit(solution)/shard_map/reduce_sum | solution.py:13
  1.7 1.0 %fusion.20 = f32[8]{0:T(128)S(1)} fusion(bf16[8,2048]{1,0:T(8,128)(2,1)} %param.19, f32[8]{0:T(128)S(1)} %broadcast_multiply_fusion.1), kind=kLoop, calls=%fused_computation.39 | loop fusion | flops 65528 | bytes 32832 | tf_op jit(solution)/shard_map/reduce_sum | solution.py:15
  3.3 0.8 %fusion.22 = bf16[8,2048]{1,0:T(8,128)(2,1)S(1)} fusion(bf16[8,2048]{1,0:T(8,128)(2,1)} %param.19, f32[2048]{0:T(1024)} %param.28, f32[8]{0:T(128)S(1)} %add_rsqrt_fusion.1, f32[8]{0:T(128)S(1)} %broadcast_multiply_fusion.1), kind=kLoop, calls=%fused_computation.41 | loop fusion | flops 81920 | bytes 73792 | tf_op jit(solution)/shard_map/convert_element_type | solution.py:60
  4.2 0.8 %convolution_bitcast_fusion = f32[8,1]{0,1:T(1,128)S(1)} fusion(bf16[8,2048]{1,0:T(8,128)(2,1)S(1)} %fusion.22, bf16[2048,1]{0,1:T(2,128)(2,1)} %param.24), kind=kOutput, calls=%fused_computation.23 | convolution fusion | flops 32768 | bytes 36896 | tf_op jit(solution)/shard_map/dot_general | solution.py:61
  5.0 0.8 %exponential_bitcast_fusion = (f32[8]{0:T(128)S(1)}, f32[8,1]{0,1:T(1,128)S(1)}) fusion(f32[8,1]{0,1:T(1,128)S(1)} %convolution_bitcast_fusion, f32[8,1]{0,1:T(1,128)} %param.32, f32[]{:T(128)} %bitcast.90, bf16[8,2048]{1,0:T(8,128)(2,1)S(1)} %fusion.22, bf16[2048,1]{0,1:T(2,128)(2,1)} %param.25), kind=kOutput, calls=%fused_computation.80 | convolution fusion | flops 32864 | bytes 36996 | tf_op jit(solution)/shard_map/dot_general | solution.py:62
  5.9 1.5 %fusion.5 = f32[8,256]{1,0:T(8,128)S(1)} fusion(bf16[8,2048]{1,0:T(8,128)(2,1)S(1)} %fusion.22, bf16[2048,256]{1,0:T(8,128)(2,1)} %param.22), kind=kOutput, calls=%fused_computation.9 | convolution fusion | flops 8392704 | bytes 1089536 | tf_op jit(solution)/shard_map/dot_general | solution.py:64
  7.4 1.4 %fusion.7 = f32[8,256]{1,0:T(8,128)S(1)} fusion(bf16[8,2048]{1,0:T(8,128)(2,1)S(1)} %fusion.22, bf16[2048,256]{1,0:T(8,128)(2,1)} %param.21, f32[8]{0:T(128)S(1)} %multiply_bitcast_fusion), kind=kOutput, calls=%fused_computation.12 | convolution fusion | flops 8394752 | bytes 1089568 | tf_op jit(solution)/shard_map/dot_general | solution.py:64
  8.8 0.4 fusion.33
  9.2 1.9 %multiply_add_fusion = f32[8,1,256,256]{3,2,1,0:T(8,128)S(1)} fusion(f32[8,1,256,256]{3,2,1,0:T(8,128)} %param.30, f32[8,256]{1,0:T(8,128)S(1)} %fusion.5, f32[8,256]{1,0:T(8,128)S(1)} %fusion.7, f32[8]{0:T(128)S(1)} %get-tuple-element.30), kind=kLoop, calls=%fused_computation.4 | loop fusion | flops 1572864 | bytes 4210720 | tf_op jit(solution)/shard_map/add | solution.py:76
  11.2 0.8 %fusion.1 = f32[8,1,256]{2,1,0:T(1,128)S(1)} fusion(f32[8,1,256,256]{3,2,1,0:T(8,128)S(1)} %multiply_add_fusion, bf16[8,256,1]{1,0,2:T(8,128)(2,1)S(1)} %bitcast.95), kind=kOutput, calls=%fused_computation.2 | convolution fusion | flops 6291456 | bytes 2109440 | tf_op jit(solution)/shard_map/shk,shkv->shv/dot_general | solution.py:80
  12.0 2.0 %fusion.23 = (f32[8,2048]{1,0:T(8,128)S(1)}, bf16[8,2048]{1,0:T(8,128)(2,1)S(1)}) fusion(bf16[8,2048]{1,0:T(8,128)(2,1)S(1)} %copy-done.3, f32[]{:T(128)S(6)} %select_n.65, bf16[256,2048]{1,0:T(8,128)(2,1)S(1)} %copy-done, bf16[8,2048]{1,0:T(8,128)(2,1)S(1)} %fusion.22, bf16[2048,256]{1,0:T(8,128)(2,1)} %param.23, f32[8,1,256]{2,1,0:T(1,128)S(1)} %fusion.1, ...), kind=kOutput, calls=%fused_computation.42 | convolution fusion | flops 16859136 | bytes 2269220 | tf_op jit(solution)/shard_map/dot_general | solution.py:84
  14.1 0.6 collective-permute-start
  14.6 0.8 %collective-permute-done = bf16[4,2048]{1,0:T(4,128)(2,1)S(1)} collective-permute-done((bf16[4,2048]{1,0:T(4,128)(2,1)S(1)}, bf16[4,2048]{1,0:T(4,128)(2,1)S(1)}, u32[]{:S(2)}, u32[]{:S(2)}) %collective-permute-start) | collective-permute-done | bytes 16416 | tf_op jit(solution)/shard_map/ppermute | solution.py:91
  15.5 0.8 %broadcast_in_dim.10 = bf16[16,4,2048]{2,1,0:T(4,128)(2,1)} broadcast(bf16[4,2048]{1,0:T(4,128)(2,1)S(1)} %fusion.26), dimensions={1,2} | broadcast | bytes 278528 | tf_op jit(solution)/shard_map/broadcast_in_dim | solution.py:93
  16.3 8.2 %all-to-all-start = ((bf16[16,4,2048]{2,1,0:T(4,128)(2,1)}), bf16[16,4,2048]{2,1,0:T(4,128)(2,1)S(1)}, u32[]{:S(2)}, u32[]{:S(2)}) async-start(bf16[16,4,2048]{2,1,0:T(4,128)(2,1)} %broadcast_in_dim.10), calls=%async_computation | async-start | bytes 524288 | tf_op jit(solution)/shard_map/all_to_all | solution.py:94
  24.5 0.5 collective-permute-start.2
  25.1 9.5 %all-to-all-done = bf16[16,4,2048]{2,1,0:T(4,128)(2,1)S(1)} async-done(((bf16[16,4,2048]{2,1,0:T(4,128)(2,1)}), bf16[16,4,2048]{2,1,0:T(4,128)(2,1)S(1)}, u32[]{:S(2)}, u32[]{:S(2)}) %all-to-all-start) | async-done | bytes 262176 | tf_op jit(solution)/shard_map/all_to_all | solution.py:94
  35.0 0.6 %div.47 = f32[32]{0:T(128)} reshape(f32[8,4]{1,0:T(8,128)S(1)} %broadcast_multiply_fusion) | data formatting | bytes 256 | tf_op jit(solution)/shard_map/div | solution.py:13
  35.8 0.2 fusion.52
  36.1 0.6 %rsqrt.22 = f32[32]{0:T(128)} reshape(f32[8,4]{1,0:T(8,128)S(1)} %add_rsqrt_fusion) | data formatting | bytes 256 | tf_op jit(solution)/shard_map/rsqrt | solution.py:16
  36.8 0.7 %copy.69 = f32[8,4]{0,1:T(4,128)} copy(f32[8,4]{1,0:T(8,128)S(1)} %add_rsqrt_fusion) | data formatting | bytes 256 | tf_op jit(solution)/shard_map/rsqrt | solution.py:16
  37.4 0.7 %constant_dynamic-slice_fusion.1 = (f32[1,4,512]{2,0,1:T(1,128)}, f32[1,4,512]{2,0,1:T(1,128)S(1)}) fusion(f32[8,4,2048]{2,0,1:T(8,128)S(1)} %get-tuple-element.34, s32[]{:T(128)S(6)} %select_n.69, s32[]{:T(128)S(6)} %select_n.71, s32[]{:T(128)S(6)} %select_n.73), kind=kLoop, calls=%fused_computation.83 | loop fusion | bytes 32780 | tf_op jit(solution)/shard_map/dynamic_slice | solution.py:102
  38.1 0.9 %multiply_convert_fusion.1 = bf16[8,4,2048]{2,0,1:T(8,128)(2,1)S(1)} fusion(f32[2048]{0:T(1024)S(1)} %copy-done.4, f32[8,4]{0,1:T(4,128)} %copy.69, f32[8,4]{0,1:T(4,128)} %copy-done.6, f32[8,4,2048]{2,1,0:T(4,128)S(1)} %bitcast_reduce_fusion), kind=kLoop, calls=%fused_computation.30 | loop fusion | flops 262144 | bytes 401664 | tf_op jit(solution)/shard_map/convert_element_type | solution.py:105
  39.1 1.2 %fusion.45 = f32[32,128]{1,0:T(8,128)S(1)} fusion(bf16[32,2048]{1,0:T(8,128)(2,1)S(1)} %convert_element_type.104, bf16[1,2048,128]{2,1,0:T(8,128)(2,1)} %param.33), kind=kOutput, calls=%fused_computation.87 | convolution fusion | flops 16777216 | bytes 671744 | tf_op jit(solution)/shard_map/dot_general | solution.py:108
  40.4 1.6 %fusion.4 = f32[32,2048]{1,0:T(8,128)S(1)} fusion(bf16[32,2048]{1,0:T(8,128)(2,1)S(1)} %convert_element_type.104, f32[32,128]{1,0:T(8,128)S(1)} %fusion.45, bf16[1,128,2048]{2,1,0:T(8,128)(2,1)} %param.35, bf16[1,2048,128]{2,1,0:T(8,128)(2,1)} %param.34), kind=kOutput, calls=%fused_computation.7 | convolution fusion | flops 33579008 | bytes 1458176 | tf_op jit(solution)/shard_map/dot_general | solution.py:111
  42.0 0.9 %fusion.50 = f32[32,128]{1,0:T(8,128)S(1)} fusion(bf16[2048,128]{1,0:T(8,128)(2,1)S(1)} %collective-permute-done.3, f32[32,2048]{1,0:T(8,128)S(1)} %reshape.311, f32[2048]{0:T(1024)S(1)} %copy-done.4, f32[32]{0:T(128)S(1)} %copy-done.8, f32[32]{0:T(128)} %div.47), kind=kOutput, calls=%fused_computation.92 | convolution fusion | flops 17039360 | bytes 811264 | tf_op jit(solution)/shard_map/dot_general | solution.py:109
  42.9 1.1 %fusion = bf16[32,2048]{1,0:T(8,128)(2,1)S(1)} fusion(f32[32,2048]{1,0:T(8,128)S(1)} %fusion.4, bf16[128,2048]{1,0:T(8,128)(2,1)S(1)} %collective-permute-done.4, f32[32,128]{1,0:T(8,128)S(1)} %fusion.50, bf16[2048,128]{1,0:T(8,128)(2,1)S(1)} %collective-permute-done.2, f32[32,2048]{1,0:T(8,128)S(1)} %reshape.311, f32[2048]{0:T(1024)S(1)} %copy-done.4, ...), kind=kOutput, calls=%fused_computation.1 | convolution fusion | flops 33972224 | bytes 1728768 | tf_op jit(solution)/shard_map/dot_general | solution.py:111
  44.1 0.7 %copy.72 = bf16[8,4,4,512]{3,1,2,0:T(4,128)(2,1)} copy(bf16[8,4,4,512]{3,2,1,0:T(4,128)(2,1)S(1)} %reshape.312) | data formatting | bytes 262144 | tf_op jit(solution)/shard_map/reshape | solution.py:116
  44.8 2.6 %all-to-all-start.1 = ((bf16[32,4,512]{2,1,0:T(4,128)(2,1)}), bf16[32,4,512]{2,1,0:T(4,128)(2,1)S(1)}, u32[]{:S(2)}, u32[]{:S(2)}) async-start(bf16[32,4,512]{2,1,0:T(4,128)(2,1)} %bitcast.22), calls=%async_computation.1 | async-start | bytes 262144 | tf_op jit(solution)/shard_map/all_to_all | solution.py:120
  47.6 0.6 %copy.74 = f32[8,1,256]{2,1,0:T(1,128)} copy(f32[8,1,256]{2,0,1:T(8,128)S(1)} %get-tuple-element.29) | data formatting | bytes 16384
  48.2 7.4 %all-to-all-done.1 = bf16[32,4,512]{2,1,0:T(4,128)(2,1)S(1)} async-done(((bf16[32,4,512]{2,1,0:T(4,128)(2,1)}), bf16[32,4,512]{2,1,0:T(4,128)(2,1)S(1)}, u32[]{:S(2)}, u32[]{:S(2)}) %all-to-all-start.1) | async-done | bytes 131104 | tf_op jit(solution)/shard_map/all_to_all | solution.py:120
  55.8 0.6 %fusion.27 = bf16[8,512]{1,0:T(8,128)(2,1)} fusion(f32[8,512]{1,0:T(8,128)S(1)} %reduce_sum.101, f32[4,512]{1,0:T(4,128)S(1)} %get-tuple-element.37, f32[4,512]{1,0:T(4,128)S(1)} %get-tuple-element.36), kind=kLoop, calls=%fused_computation.49 | loop fusion | flops 12288 | bytes 40960 | tf_op jit(solution)/shard_map/convert_element_type | solution.py:138
  (55 shorter events, 1.5 us)
Async XLA Ops:
  0.6 11.4 %copy-start = (bf16[256,2048]{1,0:T(8,128)(2,1)S(1)}, bf16[256,2048]{1,0:T(8,128)(2,1)}, u32[]{:S(2)}) copy-start(bf16[256,2048]{1,0:T(8,128)(2,1)} %param.27) | copy-start | bytes 3145732
  0.6 8.2 %copy-start.2 = (bf16[2048,256]{1,0:T(8,128)(2,1)S(1)}, bf16[2048,256]{1,0:T(8,128)(2,1)}, u32[]{:S(2)}) copy-start(bf16[2048,256]{1,0:T(8,128)(2,1)} %param.20) | copy-start | bytes 3145732
  0.7 8.2 %copy-start.7 = (f32[8,1,256]{2,1,0:T(1,128)S(1)}, f32[8,1,256]{2,1,0:T(1,128)}, u32[]{:S(2)}) copy-start(f32[8,1,256]{2,1,0:T(1,128)} %param.31) | copy-start | bytes 24580
  5.9 5.3 %copy-start.11 = (f32[8,1]{0,1:T(1,128)}, f32[8,1]{0,1:T(1,128)S(1)}, u32[]{:S(2)}) copy-start(f32[8,1]{0,1:T(1,128)S(1)} %get-tuple-element.31) | copy-start | bytes 100
  11.2 2.8 %copy-start.1 = (f32[8,1,256,256]{3,2,1,0:T(8,128)}, f32[8,1,256,256]{3,2,1,0:T(8,128)S(1)}, u32[]{:S(2)}) copy-start(f32[8,1,256,256]{3,2,1,0:T(8,128)S(1)} %multiply_add_fusion) | copy-start | bytes 6291460
  11.2 0.8 %copy-start.3 = (bf16[8,2048]{1,0:T(8,128)(2,1)S(1)}, bf16[8,2048]{1,0:T(8,128)(2,1)}, u32[]{:S(2)}) copy-start(bf16[8,2048]{1,0:T(8,128)(2,1)} %param.19) | copy-start | bytes 98308
  12.0 26.1 %copy-start.4 = (f32[2048]{0:T(1024)S(1)}, f32[2048]{0:T(1024)}, u32[]{:S(2)}) copy-start(f32[2048]{0:T(1024)} %param.29) | copy-start | bytes 24580
  14.1 1.4 %collective-permute-start = (bf16[4,2048]{1,0:T(4,128)(2,1)S(1)}, bf16[4,2048]{1,0:T(4,128)(2,1)S(1)}, u32[]{:S(2)}, u32[]{:S(2)}) collective-permute-start(bf16[4,2048]{1,0:T(4,128)(2,1)S(1)} %fusion.24), channel_id=1, source_target_pairs={{0,1},{1,0},{2,3},{3,2},{4,5},{5,4},{6,7},{7,6},{8,9},{9,8},{10,11... | collective-permute-start | bytes 49160 | tf_op jit(solution)/shard_map/ppermute | solution.py:91
  16.3 18.4 %all-to-all-start = ((bf16[16,4,2048]{2,1,0:T(4,128)(2,1)}), bf16[16,4,2048]{2,1,0:T(4,128)(2,1)S(1)}, u32[]{:S(2)}, u32[]{:S(2)}) async-start(bf16[16,4,2048]{2,1,0:T(4,128)(2,1)} %broadcast_in_dim.10), calls=%async_computation | async-start | bytes 524288 | tf_op jit(solution)/shard_map/all_to_all | solution.py:94
  24.5 17.5 %collective-permute-start.3 = (bf16[2048,128]{1,0:T(8,128)(2,1)}, bf16[2048,128]{1,0:T(8,128)(2,1)S(1)}, u32[]{:S(2)}, u32[]{:S(2)}) collective-permute-start(bf16[2048,128]{1,0:T(8,128)(2,1)} %bitcast.93), channel_id=1, source_target_pairs={{0,1},{1,0},{2,3},{3,2},{4,5},{5,4},{6,7},{7,6},{8,9},{9,8},{10,11... | collective-permute-start | bytes 1572872 | tf_op jit(solution)/shard_map/ppermute | solution.py:57
  24.5 18.4 %collective-permute-start.2 = (bf16[2048,128]{1,0:T(8,128)(2,1)}, bf16[2048,128]{1,0:T(8,128)(2,1)S(1)}, u32[]{:S(2)}, u32[]{:S(2)}) collective-permute-start(bf16[2048,128]{1,0:T(8,128)(2,1)} %bitcast.91), channel_id=1, source_target_pairs={{0,1},{1,0},{2,3},{3,2},{4,5},{5,4},{6,7},{7,6},{8,9},{9,8},{10,11... | collective-permute-start | bytes 1572872 | tf_op jit(solution)/shard_map/ppermute | solution.py:56
  25.0 17.9 %collective-permute-start.4 = (bf16[128,2048]{1,0:T(8,128)(2,1)}, bf16[128,2048]{1,0:T(8,128)(2,1)S(1)}, u32[]{:S(2)}, u32[]{:S(2)}) collective-permute-start(bf16[128,2048]{1,0:T(8,128)(2,1)} %bitcast.94), channel_id=1, source_target_pairs={{0,1},{1,0},{2,3},{3,2},{4,5},{5,4},{6,7},{7,6},{8,9},{9,8},{10,11... | collective-permute-start | bytes 1572872 | tf_op jit(solution)/shard_map/ppermute | solution.py:58
  35.0 1.1 %copy-start.6 = (f32[8,4]{0,1:T(4,128)}, f32[8,4]{0,1:T(4,128)S(1)}, u32[]{:S(2)}) copy-start(f32[8,4]{0,1:T(4,128)S(1)} %copy.67) | copy-start | bytes 388
  38.1 3.9 %copy-start.8 = (f32[32]{0:T(128)S(1)}, f32[32]{0:T(128)}, u32[]{:S(2)}) copy-start(f32[32]{0:T(128)} %rsqrt.22) | copy-start | bytes 388
  38.1 10.1 %collective-permute-start.1 = (f32[4,512]{1,0:T(4,128)S(1)}, f32[4,512]{1,0:T(4,128)S(1)}, u32[]{:S(2)}, u32[]{:S(2)}) collective-permute-start(f32[4,512]{1,0:T(4,128)S(1)} %bitcast.98), channel_id=1, source_target_pairs={{0,1},{1,0},{2,3},{3,2},{4,5},{5,4},{6,7},{7,6},{8,9},{9,8},{10,11... | collective-permute-start | bytes 24584 | tf_op jit(solution)/shard_map/ppermute | solution.py:103
  40.4 7.0 %copy-start.9 = (f32[8,4]{0,1:T(4,128)S(1)}, f32[8,4]{0,1:T(4,128)}, u32[]{:S(2)}) copy-start(f32[8,4]{0,1:T(4,128)} %param.37) | copy-start | bytes 388
  40.4 7.0 %copy-start.10 = (s32[8,4]{0,1:T(4,128)S(1)}, s32[8,4]{0,1:T(4,128)}, u32[]{:S(2)}) copy-start(s32[8,4]{0,1:T(4,128)} %param.36) | copy-start | bytes 388
  40.4 7.8 %copy-start.5 = (f32[1,4,512]{2,0,1:T(1,128)S(1)}, f32[1,4,512]{2,0,1:T(1,128)}, u32[]{:S(2)}) copy-start(f32[1,4,512]{2,0,1:T(1,128)} %get-tuple-element.32) | copy-start | bytes 24580
  44.8 10.8 %all-to-all-start.1 = ((bf16[32,4,512]{2,1,0:T(4,128)(2,1)}), bf16[32,4,512]{2,1,0:T(4,128)(2,1)S(1)}, u32[]{:S(2)}, u32[]{:S(2)}) async-start(bf16[32,4,512]{2,1,0:T(4,128)(2,1)} %bitcast.22), calls=%async_computation.1 | async-start | bytes 262144 | tf_op jit(solution)/shard_map/all_to_all | solution.py:120

commit v2 on v1

v2 whole, which is shorter than its diff:
```python
import functools
import math

import jax
import jax.numpy as jnp
from jax import lax
from jax.experimental import pallas as pl
from jax.experimental.pallas import tpu as pltpu
from jax.sharding import PartitionSpec as P


BOTH = ("ep", "tp")
F32 = jnp.float32
BF16 = jnp.bfloat16


def dot(left, right):
    return jnp.dot(left, right, preferred_element_type=F32)


def normalize(values, gain_row):
    centered = values - jnp.mean(values, -1, keepdims=True)
    variance = jnp.mean(centered * centered, -1, keepdims=True)
    return centered * lax.rsqrt(variance + 1e-05) * gain_row


def eye_mask(size):
    rows = lax.broadcasted_iota(jnp.int32, (size, size), 0)
    return rows == lax.broadcasted_iota(jnp.int32, (size, size), 1)


def as_column(row):
    size = row.shape[1]
    spread = jnp.broadcast_to(row, (size, size))
    return jnp.sum(jnp.where(eye_mask(size), spread, 0.0), axis=1, keepdims=True)


def as_row(column):
    size = column.shape[0]
    spread = jnp.broadcast_to(column, (size, size))
    return jnp.sum(jnp.where(eye_mask(size), spread, 0.0), axis=0, keepdims=True)


def cell_kernel(
    bias,
    tokens_hbm,
    gain_hbm,
    w_in_hbm,
    w_forget_hbm,
    stabilizer_hbm,
    normalizer_hbm,
    wq_hbm,
    wk_hbm,
    wv_hbm,
    memory_hbm,
    wo_hbm,
    w_out_hbm,
    routes_hbm,
    route_weight_hbm,
    sent,
    kept,
    tags,
    norm_next,
    stabilizer_next,
    keep_out,
    fresh_out,
    values_out,
    tokens,
    gain,
    w_in,
    w_forget,
    stabilizer,
    normalizer,
    wq,
    wk,
    wv,
    memory,
    wo,
    w_out,
    routes,
    route_weight,
    sems,
    *,
    experts,
):
    pairs = (
        (tokens_hbm, tokens),
        (gain_hbm, gain),
        (w_in_hbm, w_in),
        (w_forget_hbm, w_forget),
        (stabilizer_hbm, stabilizer),
        (normalizer_hbm, normalizer),
        (wq_hbm, wq),
        (wk_hbm, wk),
        (wv_hbm, wv),
        (wo_hbm, wo),
        (w_out_hbm, w_out),
        (routes_hbm, routes),
        (route_weight_hbm, route_weight),
        (memory_hbm, memory),
    )
    copies = [
        pltpu.make_async_copy(src, dst, sems.at[n]) for n, (src, dst) in enumerate(pairs)
    ]
    tp_id = lax.axis_index("tp")
    early = (0, 1, 2, 3, 4, 5, 11, 12)
    for n in early + (6, 7, 8, 13, 9, 10):
        copies[n].start()
    for n in early:
        copies[n].wait()
    seq_rows = tokens.shape[0]
    half = seq_rows // 2
    head_size = memory.shape[-1]
    token_rows = tokens[...].astype(F32)
    normed = normalize(token_rows, gain[...]).astype(BF16)
    wide = normed.astype(F32)
    gate_in = jnp.sum(wide * w_in[...].astype(F32), axis=1, keepdims=True)
    gate_forget = jnp.sum(wide * w_forget[...].astype(F32), axis=1, keepdims=True)
    logit = gate_forget + bias[0]
    log_forget = jnp.minimum(logit, 0.0) - jnp.log1p(jnp.exp(-jnp.abs(logit)))
    shifted = log_forget + as_column(stabilizer[...])
    stab = jnp.maximum(shifted, gate_in)
    keep = jnp.exp(shifted - stab)
    admit = jnp.exp(gate_in - stab)
    stabilizer_next[...] = as_row(stab)
    keep_out[...] = as_row(keep)

    def project(number, weight):
        copies[number].wait()
        return dot(normed, weight[...]).astype(BF16).astype(F32)

    queries = project(6, wq)
    columns = queries.T
    keys = project(7, wk) * (1.0 / math.sqrt(head_size))
    values = project(8, wv)
    fresh = admit * keys
    grown = keep * normalizer[...].reshape(seq_rows, head_size) + fresh
    norm_next[...] = grown.reshape(norm_next.shape)
    fresh_out[...] = fresh
    values_out[...] = values
    match = jnp.sum(queries * fresh, axis=1, keepdims=True)
    divisor = jnp.maximum(
        jnp.abs(jnp.sum(queries * grown, axis=1, keepdims=True)), jnp.exp(-stab)
    )
    named = routes[...].astype(F32)
    lanes = lax.broadcasted_iota(jnp.int32, (seq_rows, tags.shape[1]), 1)
    expert_of = (lanes % experts).astype(F32)
    share = jnp.zeros(lanes.shape, F32)
    for k in range(routes.shape[0]):
        share = share + jnp.where(
            expert_of == as_column(named[k : k + 1]), as_column(route_weight[k : k + 1]), 0.0
        )
    coarse = share.astype(BF16).astype(F32)
    share = jnp.where(lanes < experts, coarse, share - coarse)
    share = jnp.where(lanes < 2 * experts, share, 0.0).astype(BF16)
    copies[13].wait()
    recalled = []
    for s in range(seq_rows):
        recalled.append(jnp.sum(columns[:, s : s + 1] * memory[s, 0], axis=0, keepdims=True))
    old = jnp.concatenate(recalled, axis=0)
    readout = (keep * old + match * values) / divisor
    out_gate = project(9, wo)
    mixed = (jax.nn.sigmoid(out_gate) * readout).astype(BF16)
    copies[10].wait()
    head_part = dot(mixed, w_out[...])
    first = tp_id & 1 == 0
    own = head_part + jnp.where(tp_id < 2, 1.0, 0.0) * token_rows

    @pl.when(first)
    def _():
        sent[...] = head_part[half:].astype(BF16)
        kept[...] = own[:half]
        tags[...] = share[:half]

    @pl.when(jnp.logical_not(first))
    def _():
        sent[...] = head_part[:half].astype(BF16)
        kept[...] = own[half:]
        tags[...] = share[half:]


def spread_kernel(kept, met, tags, outbound):
    width = kept.shape[1]
    pair_sum = (kept[...] + met[...].astype(F32)).astype(BF16)
    for n in range(outbound.shape[0]):
        outbound[n, :, :width] = pair_sum
        outbound[n, :, width:] = tags[...]


def load_kernel(*refs):
    count = len(refs) // 2
    sems = refs[-1]
    copies = [
        pltpu.make_async_copy(refs[n], refs[count + n], sems.at[n]) for n in range(count)
    ]
    for copy in copies:
        copy.start()
    for copy in copies:
        copy.wait()


def expert_kernel(
    arrived,
    gain,
    gate_a,
    up_a,
    down_a,
    gate_b,
    up_b,
    down_b,
    blocks,
    residual,
    tags,
):
    half, quarter = blocks.shape[1:]
    width = residual.shape[1]
    rows = residual.shape[0]
    ep_size = rows // half
    duo = arrived.shape[0] // ep_size
    tp_size = width // quarter
    for e in range(ep_size):
        total = arrived[e * duo, :, :width].astype(F32)
        for x in range(1, duo):
            total = total + arrived[e * duo + x, :, :width].astype(F32)
        residual[e * half : (e + 1) * half, :] = total
        tags[e * half : (e + 1) * half, :] = arrived[e * duo, :, width:].astype(F32)
    ep_id = lax.axis_index("ep")
    lanes = lax.broadcasted_iota(jnp.int32, tags.shape, 1)
    chosen = (lanes == ep_id) | (lanes == ep_id + ep_size)
    share = jnp.sum(jnp.where(chosen, tags[...], 0.0), axis=1, keepdims=True)
    owner = lax.broadcasted_iota(jnp.int32, (rows, 1), 0) // half
    carried = jnp.where((owner == ep_id) & (lax.axis_index("tp") < 2), 1.0, 0.0)
    rows_in = normalize(residual[...], gain[...]).astype(BF16)

    def hidden(gate, up):
        both = dot(rows_in, jnp.concatenate([gate[...], up[...]], axis=1))
        gate_part, up_part = jnp.split(both, 2, axis=1)
        return (gate_part * jax.nn.sigmoid(gate_part) * up_part).astype(BF16)

    hiddens = jnp.concatenate([hidden(gate_a, up_a), hidden(gate_b, up_b)], axis=1)
    part = dot(hiddens, jnp.concatenate([down_a[...], down_b[...]], axis=0))
    part = share * part + carried * residual[...]
    for e in range(ep_size):
        for t in range(tp_size):
            piece = part[e * half : (e + 1) * half, t * quarter : (t + 1) * quarter]
            blocks[e * tp_size + t] = piece.astype(BF16)


def combine_kernel(returned, output):
    half = returned.shape[1]
    for c in range(2):
        total = returned[c].astype(F32)
        for n in range(c + 2, returned.shape[0], 2):
            total = total + returned[n].astype(F32)
        output[c * half : (c + 1) * half, :] = total.astype(BF16)


def shards(
    tokens,
    w_query,
    w_key,
    w_value,
    w_outgate,
    w_igate,
    w_fgate,
    forget_bias,
    w_out,
    gain_mix,
    gain_moe,
    memory,
    normalizer,
    stabilizer,
    expert_gate,
    expert_up,
    expert_down,
    routes,
    route_weight,
):
    ep_size = lax.axis_size("ep")
    tp_size = lax.axis_size("tp")
    seq_rows, width = tokens.shape
    head_size = memory.shape[2]
    quarter = width // tp_size
    half = seq_rows // 2
    duo = tp_size // 2
    swap = [(t, t ^ 1) for t in range(tp_size)]
    same_side = [
        [e * tp_size + x * 2 + c for e in range(ep_size) for x in range(duo)] for c in range(2)
    ]
    smem = pl.BlockSpec(memory_space=pltpu.SMEM)
    vmem = pl.BlockSpec(memory_space=pltpu.VMEM)
    hbm = pl.BlockSpec(memory_space=pltpu.HBM)

    def room(kib):
        return pltpu.CompilerParams(vmem_limit_bytes=kib * 1024)

    shape = jax.ShapeDtypeStruct
    loads = (
        tokens,
        gain_mix.reshape(1, -1),
        w_igate.T,
        w_fgate.T,
        stabilizer.T,
        normalizer,
        w_query,
        w_key,
        w_value,
        memory,
        w_outgate,
        w_out,
        routes.T,
        route_weight.T,
    )
    tag_width = -(-2 * ep_size // 128) * 128
    sent, kept, tags, norm_next, stab_row, keep, fresh, values = pl.pallas_call(
        functools.partial(cell_kernel, experts=ep_size),
        out_shape=(
            shape((half, width), BF16),
            shape((half, width), F32),
            shape((half, tag_width), BF16),
            shape(normalizer.shape, F32),
            shape((1, seq_rows), F32),
            shape((1, seq_rows), F32),
            shape((seq_rows, head_size), F32),
            shape((seq_rows, head_size), F32),
        ),
        in_specs=[smem] + [hbm] * len(loads),
        out_specs=(vmem,) * 8,
        scratch_shapes=[pltpu.VMEM(array.shape, array.dtype) for array in loads]
        + [pltpu.SemaphoreType.DMA((len(loads),))],
        compiler_params=room(20480),
        name="cell",
    )(
        forget_bias,
        *[pltpu.with_memory_space_constraint(array, pltpu.HBM) for array in loads],
    )
    weights = (expert_gate[0], expert_up[0], expert_down[0])
    sent, weights = lax.optimization_barrier((sent, weights))
    met = lax.ppermute(sent, "tp", swap)
    mates = [lax.ppermute(weight, "tp", swap) for weight in weights]
    outbound = pl.pallas_call(
        spread_kernel,
        out_shape=shape((ep_size * duo, half, width + tag_width), BF16),
        in_specs=[vmem] * 3,
        out_specs=vmem,
        compiler_params=room(8192),
        name="spread",
    )(kept, met, tags)
    arrived = lax.all_to_all(
        outbound, BOTH, 0, 0, tiled=True, axis_index_groups=same_side
    )
    memory_next = (
        keep.reshape(seq_rows, 1, 1, 1) * memory
        + fresh[:, None, :, None] * values[:, None, None, :]
    )
    owned = pl.pallas_call(
        load_kernel,
        out_shape=tuple(shape(array.shape, array.dtype) for array in weights),
        in_specs=[hbm] * 3,
        out_specs=(vmem,) * 3,
        scratch_shapes=[pltpu.SemaphoreType.DMA((3,))],
        compiler_params=room(8192),
        name="loader",
    )(*[pltpu.with_memory_space_constraint(array, pltpu.HBM) for array in weights])
    blocks = pl.pallas_call(
        expert_kernel,
        out_shape=shape((ep_size * tp_size, half, quarter), BF16),
        in_specs=[vmem] * 8,
        out_specs=vmem,
        scratch_shapes=[
            pltpu.VMEM((ep_size * half, width), F32),
            pltpu.VMEM((ep_size * half, tag_width), F32),
        ],
        compiler_params=room(24576),
        name="experts",
    )(arrived, gain_moe.reshape(1, -1), *owned, *mates)
    returned = lax.all_to_all(blocks, BOTH, 0, 0, tiled=True)
    output = pl.pallas_call(
        combine_kernel,
        out_shape=shape((seq_rows, quarter), BF16),
        in_specs=[vmem],
        out_specs=vmem,
        compiler_params=room(16384),
        name="combine",
    )(returned)
    return (output, memory_next, norm_next, stab_row.T)


def solution(mesh):
    return jax.shard_map(
        shards,
        mesh=mesh,
        in_specs=(
            P("ep", None),
            P(None, "tp"),
            P(None, "tp"),
            P(None, "tp"),
            P(None, "tp"),
            P(None, "tp"),
            P(None, "tp"),
            P("tp"),
            P("tp", None),
            P(),
            P(),
            P("ep", "tp", None, None),
            P("ep", "tp", None),
            P("ep", "tp"),
            P("ep", None, "tp"),
            P("ep", None, "tp"),
            P("ep", "tp", None),
            P("ep", None),
            P("ep", None),
        ),
        out_specs=(P("ep", "tp"), P("ep", "tp", None, None), P("ep", "tp", None), P("ep", "tp")),
        check_vma=False,
    )
```

time: 57.2 us -> 40.1 us (0.70)
  matrix products: 12.5 us -> 0 us
  Pallas kernels: 0 us -> 8.75 us
  local copies, waits for them, and re-layouts: 5.34 us -> 0.01 us
  other arithmetic: 7.17 us -> 3.27 us
  waiting for transfers between devices: 17.8 us -> 14.5 us
    dot_general x11 -> x0, matrix products: 12.5 us -> none  [the longest x3 3.27 us: shards(): jnp.dot(normed, weight, preferred_element_type=jnp.float32)]
    pallas_call x0 -> x5, Pallas kernels: none -> 8.75 us  [the longest x1 4.42 us: shards(): pl.pallas_call(functools.partial(cell_kernel, experts=ep_size), out_shape...]
    reduce_sum x8 -> x0, other arithmetic: 2.58 us -> none  [the longest x3 1.23 us: layer_norm(): row_mean = jnp.mean(values, -1, keepdims=True)]
    all_to_all x1, waiting for transfers between devices: 7.38 us -> 4.93 us  [shards(): returned = lax.all_to_all(blocks, BOTH, 0, 0, tiled=True)]
    convert_element_type x5 -> x0, other arithmetic: 2.36 us -> none  [the longest x1 0.87 us: shards(): layer_norm(residual.reshape(-1, model_width), gain_moe).astype(jnp.bfloat16)]
    add x1, other arithmetic: 1.95 us -> 3.27 us  [shards(): keep.reshape(seq_rows, 1, 1, 1) * memory]
    rsqrt x2 -> x0, local copies, waits for them, and re-layouts: 1.28 us -> none  [layer_norm(): return centered * lax.rsqrt(variance + 1e-05) * gain_vec]
    reshape x3 -> x0, local copies, waits for them, and re-layouts: 0.86 us -> none  [the longest x2 0.77 us: shards(): blocks = part.astype(jnp.bfloat16).reshape(ep_size, half, tp_size, quarte...]
  transfers between devices with their start and end apart: 7 -> 6, of which waited for: 3 -> 3; matrix products, arithmetic and copies ran while one was open for 19% -> 8% of each run, Pallas kernels for 0% -> 5%
where the time goes in v2:
time: 40.1 us; the launch traced here: 39.7 us
  waiting for transfers between devices  14.5 us (36%)
  starting transfers between devices  11.9 us (30%)
  Pallas kernels  8.75 us (22%)
  other arithmetic  3.27 us (8%)
  between operations  1.35 us (3%)
    all_to_all x1, waiting for transfers between devices, shards(): lax.all_to_all(outbound, BOTH, 0, 0, tiled=True, axis_index_groups=same_s...  9.27 us
    all_to_all x1, starting transfers between devices, shards(): lax.all_to_all(outbound, BOTH, 0, 0, tiled=True, axis_index_groups=same_s...  8.19 us
    all_to_all x1, waiting for transfers between devices, shards(): returned = lax.all_to_all(blocks, BOTH, 0, 0, tiled=True)  4.93 us
    pallas_call x1, Pallas kernels, shards(): pl.pallas_call(functools.partial(cell_kernel, experts=ep_size), out_shape...  4.42 us
    add x1, other arithmetic, shards(): keep.reshape(seq_rows, 1, 1, 1) * memory  3.27 us
    all_to_all x1, starting transfers between devices, shards(): returned = lax.all_to_all(blocks, BOTH, 0, 0, tiled=True)  2.57 us
    pallas_call x1, Pallas kernels, shards(): pl.pallas_call(expert_kernel, out_shape=shape((ep_size * tp_size, half, q...  1.59 us
    pallas_call x1, Pallas kernels, shards(): pl.pallas_call(load_kernel, out_shape=tuple((shape(array.shape, array.dty...  1.39 us
  transfers between devices with their start and end apart: 6, of which 3 were waited for; matrix products, arithmetic and copies ran while one was open for 8% of the time, Pallas kernels for 5%

profile of v2, /device:TPU:0, one launch (start us, length us, event | category | flops | bytes accessed | tf_op | source)
XLA Modules:
  0.0 39.7 jit_solution(11698629483951863609)
XLA Ops:
  1.3 4.4 %cell.1 = (bf16[4,2048]{1,0:T(4,128)(2,1)S(1)}, f32[4,2048]{1,0:T(4,128)S(1)}, bf16[4,128]{1,0:T(4,128)(2,1)S(1)}, f32[8,1,256]{2,1,0:T(1,128)}, f32[1,8]{1,0:T(...) custom-call(f32[1]{0:T(128)S(6)} %copy.23.bias, bf16[8,2048]{1,0:T(8,128)(2,1)} %tokens_hbm.1, ...), custom_call_target="tpu_custom_call" | custom-call | tf_op jit(solution)/shard_map/cell/pallas_call | solution.py:315
  5.7 0.0 copy-start
  5.7 0.6 %collective-permute-start = (bf16[4,2048]{1,0:T(4,128)(2,1)S(1)}, bf16[4,2048]{1,0:T(4,128)(2,1)S(1)}, u32[]{:S(2)}, u32[]{:S(2)}) collective-permute-start(bf16[4,2048]{1,0:T(4,128)(2,1)S(1)} %get-tuple-element.21), channel_id=1, source_target_pairs={{0,1},{1,0},{2,3},{3,2},{4,5},{5,4},{6,7},{7,6},{8,9},{9,8},{10,11... | collective-permute-start | bytes 49160 | tf_op jit(solution)/shard_map/ppermute | solution.py:339
  6.3 0.1 collective-permute-start.1
  6.4 0.4 %collective-permute-start.2 = (bf16[2048,128]{1,0:T(8,128)(2,1)}, bf16[2048,128]{1,0:T(8,128)(2,1)S(1)}, u32[]{:S(2)}, u32[]{:S(2)}) collective-permute-start(bf16[2048,128]{1,0:T(8,128)(2,1)} %bitcast.7.refs_1_), channel_id=1, source_target_pairs={{0,1},{1,0},{2,3},{3,2},{4,5},{5,4},{6,7},{7,6},{8,9},{9,8},{10,11... | collective-permute-start | bytes 1572872 | tf_op jit(solution)/shard_map/ppermute | solution.py:340
  6.8 0.1 collective-permute-start.3
  6.9 0.2 collective-permute-done.met
  7.1 0.7 %spread.1 = bf16[16,4,2176]{2,1,0:T(4,128)(2,1)} custom-call(f32[4,2048]{1,0:T(4,128)S(1)} %get-tuple-element.19.kept, bf16[4,2048]{1,0:T(4,128)(2,1)S(1)} %collective-permute-done.met, bf16[4,128]{1,0:T(4,128)(2,1)S(1)} %get-tuple-element.22.tags), custom_call_target="tpu_custom_call" | custom-call | tf_op jit(solution)/shard_map/spread/pallas_call | solution.py:341
  7.9 8.2 %all-to-all-start = ((bf16[16,4,2176]{2,1,0:T(4,128)(2,1)}), bf16[16,4,2176]{2,1,0:T(4,128)(2,1)S(1)}, u32[]{:S(2)}, u32[]{:S(2)}) async-start(bf16[16,4,2176]{2,1,0:T(4,128)(2,1)} %spread.1), calls=%async_computation | async-start | bytes 557056 | tf_op jit(solution)/shard_map/all_to_all | solution.py:349
  16.0 1.4 %loader.1 = (bf16[2048,128]{1,0:T(8,128)(2,1)S(1)}, bf16[2048,128]{1,0:T(8,128)(2,1)S(1)}, bf16[128,2048]{1,0:T(8,128)(2,1)S(1)}) custom-call(bf16[2048,128]{1,0:T(8,128)(2,1)} %bitcast.6.refs_0_, bf16[2048,128]{1,0:T(8,128)(2,1)} %bitcast.7.refs_1_, bf16[128,2048]{1,0:T(8,128)(2,1)} %bitcast.8.refs_2_), custom_call_target="tpu_custom_call" | custom-call | tf_op jit(solution)/shard_map/loader/pallas_call | solution.py:356
  17.4 0.0 collective-permute-done.1.gate_b
  17.5 0.0 collective-permute-done.2.up_b
  17.5 0.0 collective-permute-done.3.down_b
  17.5 9.3 %all-to-all-done.arrived = bf16[16,4,2176]{2,1,0:T(4,128)(2,1)S(1)} async-done(((bf16[16,4,2176]{2,1,0:T(4,128)(2,1)}), bf16[16,4,2176]{2,1,0:T(4,128)(2,1)S(1)}, u32[]{:S(2)}, u32[]{:S(2)}) %all-to-all-start) | async-done | bytes 278560 | tf_op jit(solution)/shard_map/all_to_all | solution.py:349
  26.7 0.0 copy-done
  26.7 1.6 %experts.1 = bf16[32,4,512]{2,1,0:T(4,128)(2,1)} custom-call(bf16[16,4,2176]{2,1,0:T(4,128)(2,1)S(1)} %all-to-all-done.arrived, f32[1,2048]{1,0:T(1,128)S(1)} %bitcast.12, bf16[2048,128]{1,0:T(8,128)(2,1)S(1)} %get-tuple-element.26.gate_a, bf16[2048,128]{1,0:T(8,128)(2,1)S(1)} %get-tuple-element.27.up_a, bf16[128,2048]{1,0:T(8,128)(2,1)S(1)} %get-tuple-element.28.down_a, ...), custom_call_target="tpu_custom_call" | custom-call | tf_op jit(solution)/shard_map/experts/pallas_call | solution.py:365
  28.3 2.6 %all-to-all-start.1 = ((bf16[32,4,512]{2,1,0:T(4,128)(2,1)}), bf16[32,4,512]{2,1,0:T(4,128)(2,1)S(1)}, u32[]{:S(2)}, u32[]{:S(2)}) async-start(bf16[32,4,512]{2,1,0:T(4,128)(2,1)} %experts.1), calls=%async_computation.1 | async-start | bytes 262144 | tf_op jit(solution)/shard_map/all_to_all | solution.py:377
  30.9 3.3 %multiply_add_fusion = f32[8,1,256,256]{3,2,1,0:T(8,128)} fusion(f32[8,1,256,256]{3,2,1,0:T(8,128)} %memory_hbm.1, f32[8,256]{1,0:T(8,128)S(1)} %get-tuple-element.31, f32[8,256]{1,0:T(8,128)S(1)} %get-tuple-element.30, f32[8]{0:T(128)S(1)} %bitcast.13), kind=kLoop, calls=%fused_computation | loop fusion | flops 1572864 | bytes 4210720 | tf_op jit(solution)/shard_map/add | solution.py:353
  34.2 4.9 %all-to-all-done.1.returned = bf16[32,4,512]{2,1,0:T(4,128)(2,1)S(1)} async-done(((bf16[32,4,512]{2,1,0:T(4,128)(2,1)}), bf16[32,4,512]{2,1,0:T(4,128)(2,1)S(1)}, u32[]{:S(2)}, u32[]{:S(2)}) %all-to-all-start.1) | async-done | bytes 131104 | tf_op jit(solution)/shard_map/all_to_all | solution.py:377
  39.1 0.6 %combine.1 = bf16[8,512]{1,0:T(8,128)(2,1)} custom-call(bf16[32,4,512]{2,1,0:T(4,128)(2,1)S(1)} %all-to-all-done.1.returned), custom_call_target="tpu_custom_call" | custom-call | tf_op jit(solution)/shard_map/combine/pallas_call | solution.py:378
Async XLA Ops:
  5.7 21.0 %copy-start = (f32[2048]{0:T(1024)S(1)}, f32[2048]{0:T(1024)}, u32[]{:S(2)}) copy-start(f32[2048]{0:T(1024)} %param.29) | copy-start | bytes 24580
  5.7 1.4 %collective-permute-start = (bf16[4,2048]{1,0:T(4,128)(2,1)S(1)}, bf16[4,2048]{1,0:T(4,128)(2,1)S(1)}, u32[]{:S(2)}, u32[]{:S(2)}) collective-permute-start(bf16[4,2048]{1,0:T(4,128)(2,1)S(1)} %get-tuple-element.21), channel_id=1, source_target_pairs={{0,1},{1,0},{2,3},{3,2},{4,5},{5,4},{6,7},{7,6},{8,9},{9,8},{10,11... | collective-permute-start | bytes 49160 | tf_op jit(solution)/shard_map/ppermute | solution.py:339
  6.3 11.2 %collective-permute-start.1 = (bf16[2048,128]{1,0:T(8,128)(2,1)}, bf16[2048,128]{1,0:T(8,128)(2,1)S(1)}, u32[]{:S(2)}, u32[]{:S(2)}) collective-permute-start(bf16[2048,128]{1,0:T(8,128)(2,1)} %bitcast.6.refs_0_), channel_id=1, source_target_pairs={{0,1},{1,0},{2,3},{3,2},{4,5},{5,4},{6,7},{7,6},{8,9},{9,8},{10,11... | collective-permute-start | bytes 1572872 | tf_op jit(solution)/shard_map/ppermute | solution.py:340
  6.4 11.1 %collective-permute-start.2 = (bf16[2048,128]{1,0:T(8,128)(2,1)}, bf16[2048,128]{1,0:T(8,128)(2,1)S(1)}, u32[]{:S(2)}, u32[]{:S(2)}) collective-permute-start(bf16[2048,128]{1,0:T(8,128)(2,1)} %bitcast.7.refs_1_), channel_id=1, source_target_pairs={{0,1},{1,0},{2,3},{3,2},{4,5},{5,4},{6,7},{7,6},{8,9},{9,8},{10,11... | collective-permute-start | bytes 1572872 | tf_op jit(solution)/shard_map/ppermute | solution.py:340
  6.8 10.7 %collective-permute-start.3 = (bf16[128,2048]{1,0:T(8,128)(2,1)}, bf16[128,2048]{1,0:T(8,128)(2,1)S(1)}, u32[]{:S(2)}, u32[]{:S(2)}) collective-permute-start(bf16[128,2048]{1,0:T(8,128)(2,1)} %bitcast.8.refs_2_), channel_id=1, source_target_pairs={{0,1},{1,0},{2,3},{3,2},{4,5},{5,4},{6,7},{7,6},{8,9},{9,8},{10,11... | collective-permute-start | bytes 1572872 | tf_op jit(solution)/shard_map/ppermute | solution.py:340
  7.9 18.9 %all-to-all-start = ((bf16[16,4,2176]{2,1,0:T(4,128)(2,1)}), bf16[16,4,2176]{2,1,0:T(4,128)(2,1)S(1)}, u32[]{:S(2)}, u32[]{:S(2)}) async-start(bf16[16,4,2176]{2,1,0:T(4,128)(2,1)} %spread.1), calls=%async_computation | async-start | bytes 557056 | tf_op jit(solution)/shard_map/all_to_all | solution.py:349
  28.3 10.8 %all-to-all-start.1 = ((bf16[32,4,512]{2,1,0:T(4,128)(2,1)}), bf16[32,4,512]{2,1,0:T(4,128)(2,1)S(1)}, u32[]{:S(2)}, u32[]{:S(2)}) async-start(bf16[32,4,512]{2,1,0:T(4,128)(2,1)} %experts.1), calls=%async_computation.1 | async-start | bytes 262144 | tf_op jit(solution)/shard_map/all_to_all | solution.py:377

commit v3 on v2

--- a/solution.py
+++ b/solution.py
@@ -59,9 +59,11 @@
     route_weight_hbm,
     sent,
     kept,
-    tags,
-    norm_next,
-    stabilizer_next,
+    factors_out,
+    row_factor,
+    row_carry,
+    norm_hbm,
+    stabilizer_next_hbm,
     keep_out,
     fresh_out,
     values_out,
@@ -79,9 +81,10 @@
     w_out,
     routes,
     route_weight,
+    norm_next,
+    stabilizer_next,
     sems,
-    *,
-    experts,
+    write_sems,
 ):
     pairs = (
         (tokens_hbm, tokens),
@@ -103,6 +106,7 @@
         pltpu.make_async_copy(src, dst, sems.at[n]) for n, (src, dst) in enumerate(pairs)
     ]
     tp_id = lax.axis_index("tp")
+    ep_id = lax.axis_index("ep")
     early = (0, 1, 2, 3, 4, 5, 11, 12)
     for n in early + (6, 7, 8, 13, 9, 10):
         copies[n].start()
@@ -124,6 +128,11 @@
     admit = jnp.exp(gate_in - stab)
     stabilizer_next[...] = as_row(stab)
     keep_out[...] = as_row(keep)
+    writes = [
+        pltpu.make_async_copy(stabilizer_next, stabilizer_next_hbm, write_sems.at[0]),
+        pltpu.make_async_copy(norm_next, norm_hbm, write_sems.at[1]),
+    ]
+    writes[0].start()
 
     def project(number, weight):
         copies[number].wait()
@@ -136,6 +145,7 @@
     fresh = admit * keys
     grown = keep * normalizer[...].reshape(seq_rows, head_size) + fresh
     norm_next[...] = grown.reshape(norm_next.shape)
+    writes[1].start()
     fresh_out[...] = fresh
     values_out[...] = values
     match = jnp.sum(queries * fresh, axis=1, keepdims=True)
@@ -143,16 +153,21 @@
         jnp.abs(jnp.sum(queries * grown, axis=1, keepdims=True)), jnp.exp(-stab)
     )
     named = routes[...].astype(F32)
-    lanes = lax.broadcasted_iota(jnp.int32, (seq_rows, tags.shape[1]), 1)
-    expert_of = (lanes % experts).astype(F32)
+    lanes = lax.broadcasted_iota(jnp.int32, factors_out.shape, 1)
+    expert_of = lanes.astype(F32)
     share = jnp.zeros(lanes.shape, F32)
     for k in range(routes.shape[0]):
         share = share + jnp.where(
             expert_of == as_column(named[k : k + 1]), as_column(route_weight[k : k + 1]), 0.0
         )
-    coarse = share.astype(BF16).astype(F32)
-    share = jnp.where(lanes < experts, coarse, share - coarse)
-    share = jnp.where(lanes < 2 * experts, share, 0.0).astype(BF16)
+    factors_out[...] = jnp.where(lanes == ep_id, 1.0, share)
+    local = jnp.sum(jnp.where(lanes == ep_id, share, 0.0), axis=1, keepdims=True)
+    local = jnp.where(tp_id & 1 == 0, local[:half], local[half:])
+    row_count = row_factor.shape[0]
+    local = jnp.concatenate([local] * (row_count // half), axis=0)
+    owned = lax.broadcasted_iota(jnp.int32, row_factor.shape, 0) // half == ep_id
+    row_factor[...] = jnp.where(owned, local, 1.0)
+    row_carry[...] = jnp.where(owned & (tp_id < 2), 1.0, 0.0)
     copies[13].wait()
     recalled = []
     for s in range(seq_rows):
@@ -170,21 +185,20 @@
     def _():
         sent[...] = head_part[half:].astype(BF16)
         kept[...] = own[:half]
-        tags[...] = share[:half]
 
     @pl.when(jnp.logical_not(first))
     def _():
         sent[...] = head_part[:half].astype(BF16)
         kept[...] = own[half:]
-        tags[...] = share[half:]
-
-
-def spread_kernel(kept, met, tags, outbound):
-    width = kept.shape[1]
+
+    for write in writes:
+        write.wait()
+
+
+def spread_kernel(kept, met, outbound):
     pair_sum = (kept[...] + met[...].astype(F32)).astype(BF16)
     for n in range(outbound.shape[0]):
-        outbound[n, :, :width] = pair_sum
-        outbound[n, :, width:] = tags[...]
+        outbound[n] = pair_sum
 
 
 def load_kernel(*refs):
@@ -201,6 +215,8 @@
 
 def expert_kernel(
     arrived,
+    row_factor,
+    row_carry,
     gain,
     gate_a,
     up_a,
@@ -210,26 +226,17 @@
     down_b,
     blocks,
     residual,
-    tags,
 ):
     half, quarter = blocks.shape[1:]
-    width = residual.shape[1]
-    rows = residual.shape[0]
+    rows, width = residual.shape
     ep_size = rows // half
     duo = arrived.shape[0] // ep_size
     tp_size = width // quarter
     for e in range(ep_size):
-        total = arrived[e * duo, :, :width].astype(F32)
+        total = arrived[e * duo].astype(F32)
         for x in range(1, duo):
-            total = total + arrived[e * duo + x, :, :width].astype(F32)
+            total = total + arrived[e * duo + x].astype(F32)
         residual[e * half : (e + 1) * half, :] = total
-        tags[e * half : (e + 1) * half, :] = arrived[e * duo, :, width:].astype(F32)
-    ep_id = lax.axis_index("ep")
-    lanes = lax.broadcasted_iota(jnp.int32, tags.shape, 1)
-    chosen = (lanes == ep_id) | (lanes == ep_id + ep_size)
-    share = jnp.sum(jnp.where(chosen, tags[...], 0.0), axis=1, keepdims=True)
-    owner = lax.broadcasted_iota(jnp.int32, (rows, 1), 0) // half
-    carried = jnp.where((owner == ep_id) & (lax.axis_index("tp") < 2), 1.0, 0.0)
     rows_in = normalize(residual[...], gain[...]).astype(BF16)
 
     def hidden(gate, up):
@@ -239,20 +246,25 @@
 
     hiddens = jnp.concatenate([hidden(gate_a, up_a), hidden(gate_b, up_b)], axis=1)
     part = dot(hiddens, jnp.concatenate([down_a[...], down_b[...]], axis=0))
-    part = share * part + carried * residual[...]
+    part = row_factor[:, :1] * part + row_carry[:, :1] * residual[...]
     for e in range(ep_size):
         for t in range(tp_size):
             piece = part[e * half : (e + 1) * half, t * quarter : (t + 1) * quarter]
             blocks[e * tp_size + t] = piece.astype(BF16)
 
 
-def combine_kernel(returned, output):
+def combine_kernel(returned, factors, output, *, ep_size):
     half = returned.shape[1]
+    tp_size = returned.shape[0] // ep_size
     for c in range(2):
-        total = returned[c].astype(F32)
-        for n in range(c + 2, returned.shape[0], 2):
-            total = total + returned[n].astype(F32)
-        output[c * half : (c + 1) * half, :] = total.astype(BF16)
+        rows = slice(c * half, (c + 1) * half)
+        total = 0.0
+        for e in range(ep_size):
+            value = returned[e * tp_size + c].astype(F32)
+            for x in range(1, tp_size // 2):
+                value = value + returned[e * tp_size + 2 * x + c].astype(F32)
+            total = total + factors[rows, e : e + 1] * value
+        output[rows, :] = total.astype(BF16)
 
 
 def shards(
@@ -311,13 +323,15 @@
         routes.T,
         route_weight.T,
     )
-    tag_width = -(-2 * ep_size // 128) * 128
-    sent, kept, tags, norm_next, stab_row, keep, fresh, values = pl.pallas_call(
-        functools.partial(cell_kernel, experts=ep_size),
+    lane_width = -(-ep_size // 128) * 128
+    sent, kept, factors, row_factor, row_carry, norm_next, stab_row, keep, fresh, values = pl.pallas_call(
+        cell_kernel,
         out_shape=(
             shape((half, width), BF16),
             shape((half, width), F32),
-            shape((half, tag_width), BF16),
+            shape((seq_rows, lane_width), F32),
+            shape((ep_size * half, 128), F32),
+            shape((ep_size * half, 128), F32),
             shape(normalizer.shape, F32),
             shape((1, seq_rows), F32),
             shape((1, seq_rows), F32),
@@ -325,9 +339,14 @@
             shape((seq_rows, head_size), F32),
         ),
         in_specs=[smem] + [hbm] * len(loads),
-        out_specs=(vmem,) * 8,
+        out_specs=(vmem,) * 5 + (hbm,) * 2 + (vmem,) * 3,
         scratch_shapes=[pltpu.VMEM(array.shape, array.dtype) for array in loads]
-        + [pltpu.SemaphoreType.DMA((len(loads),))],
+        + [
+            pltpu.VMEM(normalizer.shape, F32),
+            pltpu.VMEM((1, seq_rows), F32),
+            pltpu.SemaphoreType.DMA((len(loads),)),
+            pltpu.SemaphoreType.DMA((2,)),
+        ],
         compiler_params=room(20480),
         name="cell",
     )(
@@ -340,12 +359,12 @@
     mates = [lax.ppermute(weight, "tp", swap) for weight in weights]
     outbound = pl.pallas_call(
         spread_kernel,
-        out_shape=shape((ep_size * duo, half, width + tag_width), BF16),
-        in_specs=[vmem] * 3,
+        out_shape=shape((ep_size * duo, half, width), BF16),
+        in_specs=[vmem] * 2,
         out_specs=vmem,
         compiler_params=room(8192),
         name="spread",
-    )(kept, met, tags)
+    )(kept, met)
     arrived = lax.all_to_all(
         outbound, BOTH, 0, 0, tiled=True, axis_index_groups=same_side
     )
@@ -365,24 +384,21 @@
     blocks = pl.pallas_call(
         expert_kernel,
         out_shape=shape((ep_size * tp_size, half, quarter), BF16),
-        in_specs=[vmem] * 8,
+        in_specs=[vmem] * 10,
         out_specs=vmem,
-        scratch_shapes=[
-            pltpu.VMEM((ep_size * half, width), F32),
-            pltpu.VMEM((ep_size * half, tag_width), F32),
-        ],
+        scratch_shapes=[pltpu.VMEM((ep_size * half, width), F32)],
         compiler_params=room(24576),
         name="experts",
-    )(arrived, gain_moe.reshape(1, -1), *owned, *mates)
+    )(arrived, row_factor, row_carry, gain_moe.reshape(1, -1), *owned, *mates)
     returned = lax.all_to_all(blocks, BOTH, 0, 0, tiled=True)
     output = pl.pallas_call(
-        combine_kernel,
+        functools.partial(combine_kernel, ep_size=ep_size),
         out_shape=shape((seq_rows, quarter), BF16),
-        in_specs=[vmem],
+        in_specs=[vmem] * 2,
         out_specs=vmem,
         compiler_params=room(16384),
         name="combine",
-    )(returned)
+    )(returned, factors)
     return (output, memory_next, norm_next, stab_row.T)
 
 

time: 40.1 us -> 41.5 us (1.035)
  waiting for transfers between devices: 14.5 us -> 16.4 us
  Pallas kernels: 8.75 us -> 8.23 us
    ppermute x1, waiting for transfers between devices: 0.25 us -> 2.68 us  [shards(): met = lax.ppermute(sent, 'tp', swap)]
    pallas_call x2, Pallas kernels: 5.04 us -> 4.53 us  [the longest x1 3.83 us: shards(): pl.pallas_call(cell_kernel, out_shape=(shape((half, width), BF16), shape(...]
    all_to_all x1, waiting for transfers between devices: 9.27 us -> 8.78 us  [shards(): lax.all_to_all(outbound, BOTH, 0, 0, tiled=True, axis_index_groups=same_s...]
    ppermute x3, starting transfers between devices: 0.59 us -> 1.07 us  [shards(): mates = [lax.ppermute(weight, 'tp', swap) for weight in weights]]
    ppermute x1, starting transfers between devices: 0.56 us -> 0.08 us  [shards(): met = lax.ppermute(sent, 'tp', swap)]
where the time goes in v3:
time: 41.5 us; the launch traced here: 41.2 us
  waiting for transfers between devices  16.4 us (40%)
  starting transfers between devices  11.9 us (29%)
  Pallas kernels  8.23 us (20%)
  other arithmetic  3.27 us (8%)
  between operations  1.34 us (3%)
    all_to_all x1, waiting for transfers between devices, shards(): lax.all_to_all(outbound, BOTH, 0, 0, tiled=True, axis_index_groups=same_s...  8.78 us
    all_to_all x1, starting transfers between devices, shards(): lax.all_to_all(outbound, BOTH, 0, 0, tiled=True, axis_index_groups=same_s...  8.22 us
    all_to_all x1, waiting for transfers between devices, shards(): returned = lax.all_to_all(blocks, BOTH, 0, 0, tiled=True)  4.93 us
    pallas_call x1, Pallas kernels, shards(): pl.pallas_call(cell_kernel, out_shape=(shape((half, width), BF16), shape(...  3.83 us
    add x1, other arithmetic, shards(): keep.reshape(seq_rows, 1, 1, 1) * memory  3.27 us
    ppermute x1, waiting for transfers between devices, shards(): met = lax.ppermute(sent, 'tp', swap)  2.68 us
    all_to_all x1, starting transfers between devices, shards(): returned = lax.all_to_all(blocks, BOTH, 0, 0, tiled=True)  2.57 us
    pallas_call x1, Pallas kernels, shards(): pl.pallas_call(expert_kernel, out_shape=shape((ep_size * tp_size, half, q...  1.59 us
  transfers between devices with their start and end apart: 6, of which 3 were waited for; matrix products, arithmetic and copies ran while one was open for 8% of the time, Pallas kernels for 5%

profile of v3, /device:TPU:0, one launch (start us, length us, event | category | flops | bytes accessed | tf_op | source)
XLA Modules:
  0.0 41.2 jit_solution(9415191932709844219)
XLA Ops:
  1.3 3.8 %cell.1 = (bf16[4,2048]{1,0:T(4,128)(2,1)S(1)}, f32[4,2048]{1,0:T(4,128)S(1)}, f32[8,128]{1,0:T(8,128)S(1)}, f32[32,128]{1,0:T(8,128)S(1)}, f32[32,128]{1,0:T(8,...) custom-call(f32[1]{0:T(128)S(6)} %copy.23.bias, ...), custom_call_target="tpu_custom_call" | custom-call | tf_op jit(solution)/shard_map/cell/pallas_call | solution.py:327
  5.1 0.0 copy-start
  5.1 0.6 %collective-permute-start.1 = (bf16[2048,128]{1,0:T(8,128)(2,1)}, bf16[2048,128]{1,0:T(8,128)(2,1)S(1)}, u32[]{:S(2)}, u32[]{:S(2)}) collective-permute-start(bf16[2048,128]{1,0:T(8,128)(2,1)} %bitcast.6.refs_0_), channel_id=1, source_target_pairs={{0,1},{1,0},{2,3},{3,2},{4,5},{5,4},{6,7},{7,6},{8,9},{9,8},{10,11... | collective-permute-start | bytes 1572872 | tf_op jit(solution)/shard_map/ppermute | solution.py:359
  5.7 0.1 collective-permute-start.2
  5.8 0.4 %collective-permute-start.3 = (bf16[128,2048]{1,0:T(8,128)(2,1)}, bf16[128,2048]{1,0:T(8,128)(2,1)S(1)}, u32[]{:S(2)}, u32[]{:S(2)}) collective-permute-start(bf16[128,2048]{1,0:T(8,128)(2,1)} %bitcast.8.refs_2_), channel_id=1, source_target_pairs={{0,1},{1,0},{2,3},{3,2},{4,5},{5,4},{6,7},{7,6},{8,9},{9,8},{10,11... | collective-permute-start | bytes 1572872 | tf_op jit(solution)/shard_map/ppermute | solution.py:359
  6.2 0.1 collective-permute-start
  6.3 2.7 %collective-permute-done.met = bf16[4,2048]{1,0:T(4,128)(2,1)S(1)} collective-permute-done((bf16[4,2048]{1,0:T(4,128)(2,1)S(1)}, bf16[4,2048]{1,0:T(4,128)(2,1)S(1)}, u32[]{:S(2)}, u32[]{:S(2)}) %collective-permute-start) | collective-permute-done | bytes 16416 | tf_op jit(solution)/shard_map/ppermute | solution.py:358
  9.0 0.7 %spread.1 = bf16[16,4,2048]{2,1,0:T(4,128)(2,1)} custom-call(f32[4,2048]{1,0:T(4,128)S(1)} %get-tuple-element.21.kept, bf16[4,2048]{1,0:T(4,128)(2,1)S(1)} %collective-permute-done.met), custom_call_target="tpu_custom_call" | custom-call | tf_op jit(solution)/shard_map/spread/pallas_call | solution.py:360
  9.7 8.2 %all-to-all-start = ((bf16[16,4,2048]{2,1,0:T(4,128)(2,1)}), bf16[16,4,2048]{2,1,0:T(4,128)(2,1)S(1)}, u32[]{:S(2)}, u32[]{:S(2)}) async-start(bf16[16,4,2048]{2,1,0:T(4,128)(2,1)} %spread.1), calls=%async_computation | async-start | bytes 524288 | tf_op jit(solution)/shard_map/all_to_all | solution.py:368
  17.9 1.4 %loader.1 = (bf16[2048,128]{1,0:T(8,128)(2,1)S(1)}, bf16[2048,128]{1,0:T(8,128)(2,1)S(1)}, bf16[128,2048]{1,0:T(8,128)(2,1)S(1)}) custom-call(bf16[2048,128]{1,0:T(8,128)(2,1)} %bitcast.6.refs_0_, bf16[2048,128]{1,0:T(8,128)(2,1)} %bitcast.7.refs_1_, bf16[128,2048]{1,0:T(8,128)(2,1)} %bitcast.8.refs_2_), custom_call_target="tpu_custom_call" | custom-call | tf_op jit(solution)/shard_map/loader/pallas_call | solution.py:375
  19.3 8.8 %all-to-all-done.arrived = bf16[16,4,2048]{2,1,0:T(4,128)(2,1)S(1)} async-done(((bf16[16,4,2048]{2,1,0:T(4,128)(2,1)}), bf16[16,4,2048]{2,1,0:T(4,128)(2,1)S(1)}, u32[]{:S(2)}, u32[]{:S(2)}) %all-to-all-start) | async-done | bytes 262176 | tf_op jit(solution)/shard_map/all_to_all | solution.py:368
  28.1 0.0 collective-permute-done.1.gate_b
  28.1 0.0 collective-permute-done.2.up_b
  28.1 0.0 collective-permute-done.3.down_b
  28.1 0.0 copy-done
  28.1 1.6 %experts.1 = bf16[32,4,512]{2,1,0:T(4,128)(2,1)} custom-call(bf16[16,4,2048]{2,1,0:T(4,128)(2,1)S(1)} %all-to-all-done.arrived, f32[32,128]{1,0:T(8,128)S(1)} %get-tuple-element.24.row_factor, f32[32,128]{1,0:T(8,128)S(1)} %get-tuple-element.25.row_carry, f32[1,2048]{1,0:T(1,128)S(1)} %bitcast.12, bf16[2048,128]{1,0:T(8,128)(2,1)S(1)} %get-tuple-element.29.gate_a, ...), custom_call_target="tpu_custom_call" | custom-call | tf_op jit(solution)/shard_map/experts/pallas_call | solution.py:384
  29.7 2.6 %all-to-all-start.1 = ((bf16[32,4,512]{2,1,0:T(4,128)(2,1)}), bf16[32,4,512]{2,1,0:T(4,128)(2,1)S(1)}, u32[]{:S(2)}, u32[]{:S(2)}) async-start(bf16[32,4,512]{2,1,0:T(4,128)(2,1)} %experts.1), calls=%async_computation.1 | async-start | bytes 262144 | tf_op jit(solution)/shard_map/all_to_all | solution.py:393
  32.3 3.3 %multiply_add_fusion = f32[8,1,256,256]{3,2,1,0:T(8,128)} fusion(f32[8,1,256,256]{3,2,1,0:T(8,128)} %memory_hbm.1, f32[8,256]{1,0:T(8,128)S(1)} %get-tuple-element.35, f32[8,256]{1,0:T(8,128)S(1)} %get-tuple-element.34, f32[8]{0:T(128)S(1)} %bitcast.13), kind=kLoop, calls=%fused_computation | loop fusion | flops 1572864 | bytes 4210720 | tf_op jit(solution)/shard_map/add | solution.py:372
  35.6 4.9 %all-to-all-done.1.returned = bf16[32,4,512]{2,1,0:T(4,128)(2,1)S(1)} async-done(((bf16[32,4,512]{2,1,0:T(4,128)(2,1)}), bf16[32,4,512]{2,1,0:T(4,128)(2,1)S(1)}, u32[]{:S(2)}, u32[]{:S(2)}) %all-to-all-start.1) | async-done | bytes 131104 | tf_op jit(solution)/shard_map/all_to_all | solution.py:393
  40.5 0.7 %combine.1 = bf16[8,512]{1,0:T(8,128)(2,1)} custom-call(bf16[32,4,512]{2,1,0:T(4,128)(2,1)S(1)} %all-to-all-done.1.returned, f32[8,128]{1,0:T(8,128)S(1)} %get-tuple-element.32.factors), custom_call_target="tpu_custom_call" | custom-call | tf_op jit(solution)/shard_map/combine/pallas_call | solution.py:394
Async XLA Ops:
  5.1 23.0 %copy-start = (f32[2048]{0:T(1024)S(1)}, f32[2048]{0:T(1024)}, u32[]{:S(2)}) copy-start(f32[2048]{0:T(1024)} %param.29) | copy-start | bytes 24580
  5.1 23.0 %collective-permute-start.1 = (bf16[2048,128]{1,0:T(8,128)(2,1)}, bf16[2048,128]{1,0:T(8,128)(2,1)S(1)}, u32[]{:S(2)}, u32[]{:S(2)}) collective-permute-start(bf16[2048,128]{1,0:T(8,128)(2,1)} %bitcast.6.refs_0_), channel_id=1, source_target_pairs={{0,1},{1,0},{2,3},{3,2},{4,5},{5,4},{6,7},{7,6},{8,9},{9,8},{10,11... | collective-permute-start | bytes 1572872 | tf_op jit(solution)/shard_map/ppermute | solution.py:359
  5.7 22.4 %collective-permute-start.2 = (bf16[2048,128]{1,0:T(8,128)(2,1)}, bf16[2048,128]{1,0:T(8,128)(2,1)S(1)}, u32[]{:S(2)}, u32[]{:S(2)}) collective-permute-start(bf16[2048,128]{1,0:T(8,128)(2,1)} %bitcast.7.refs_1_), channel_id=1, source_target_pairs={{0,1},{1,0},{2,3},{3,2},{4,5},{5,4},{6,7},{7,6},{8,9},{9,8},{10,11... | collective-permute-start | bytes 1572872 | tf_op jit(solution)/shard_map/ppermute | solution.py:359
  5.8 22.3 %collective-permute-start.3 = (bf16[128,2048]{1,0:T(8,128)(2,1)}, bf16[128,2048]{1,0:T(8,128)(2,1)S(1)}, u32[]{:S(2)}, u32[]{:S(2)}) collective-permute-start(bf16[128,2048]{1,0:T(8,128)(2,1)} %bitcast.8.refs_2_), channel_id=1, source_target_pairs={{0,1},{1,0},{2,3},{3,2},{4,5},{5,4},{6,7},{7,6},{8,9},{9,8},{10,11... | collective-permute-start | bytes 1572872 | tf_op jit(solution)/shard_map/ppermute | solution.py:359
  6.2 2.8 %collective-permute-start = (bf16[4,2048]{1,0:T(4,128)(2,1)S(1)}, bf16[4,2048]{1,0:T(4,128)(2,1)S(1)}, u32[]{:S(2)}, u32[]{:S(2)}) collective-permute-start(bf16[4,2048]{1,0:T(4,128)(2,1)S(1)} %get-tuple-element.23), channel_id=1, source_target_pairs={{0,1},{1,0},{2,3},{3,2},{4,5},{5,4},{6,7},{7,6},{8,9},{9,8},{10,11... | collective-permute-start | bytes 49160 | tf_op jit(solution)/shard_map/ppermute | solution.py:358
  9.7 18.4 %all-to-all-start = ((bf16[16,4,2048]{2,1,0:T(4,128)(2,1)}), bf16[16,4,2048]{2,1,0:T(4,128)(2,1)S(1)}, u32[]{:S(2)}, u32[]{:S(2)}) async-start(bf16[16,4,2048]{2,1,0:T(4,128)(2,1)} %spread.1), calls=%async_computation | async-start | bytes 524288 | tf_op jit(solution)/shard_map/all_to_all | solution.py:368
  29.7 10.8 %all-to-all-start.1 = ((bf16[32,4,512]{2,1,0:T(4,128)(2,1)}), bf16[32,4,512]{2,1,0:T(4,128)(2,1)S(1)}, u32[]{:S(2)}, u32[]{:S(2)}) async-start(bf16[32,4,512]{2,1,0:T(4,128)(2,1)} %experts.1), calls=%async_computation.1 | async-start | bytes 262144 | tf_op jit(solution)/shard_map/all_to_all | solution.py:393

commit v4 on v3

--- a/solution.py
+++ b/solution.py
@@ -57,7 +57,48 @@
     w_out_hbm,
     routes_hbm,
     route_weight_hbm,
-    sent,
+    *rest,
+    tp_size,
+):
+    sents, rest = rest[: tp_size - 1], rest[tp_size - 1 :]
+    cell_body(
+        bias,
+        tokens_hbm,
+        gain_hbm,
+        w_in_hbm,
+        w_forget_hbm,
+        stabilizer_hbm,
+        normalizer_hbm,
+        wq_hbm,
+        wk_hbm,
+        wv_hbm,
+        memory_hbm,
+        wo_hbm,
+        w_out_hbm,
+        routes_hbm,
+        route_weight_hbm,
+        sents,
+        *rest,
+    )
+
+
+def cell_body(
+    bias,
+    tokens_hbm,
+    gain_hbm,
+    w_in_hbm,
+    w_forget_hbm,
+    stabilizer_hbm,
+    normalizer_hbm,
+    wq_hbm,
+    wk_hbm,
+    wv_hbm,
+    memory_hbm,
+    wo_hbm,
+    w_out_hbm,
+    routes_hbm,
+    route_weight_hbm,
+    sents,
     kept,
     factors_out,
     row_factor,
@@ -113,7 +154,8 @@
     for n in early:
         copies[n].wait()
     seq_rows = tokens.shape[0]
-    half = seq_rows // 2
+    tp_size = len(sents) + 1
+    portion = seq_rows // tp_size
     head_size = memory.shape[-1]
     token_rows = tokens[...].astype(F32)
     normed = normalize(token_rows, gain[...]).astype(BF16)
@@ -160,14 +202,23 @@
         share = share + jnp.where(
             expert_of == as_column(named[k : k + 1]), as_column(route_weight[k : k + 1]), 0.0
         )
-    factors_out[...] = jnp.where(lanes == ep_id, 1.0, share)
+
+    def side(array, c):
+        return [array[portion * t : portion * (t + 1)] for t in range(c, tp_size, 2)]
+
+    factors = jnp.where(lanes == ep_id, 1.0, share)
+    factors_out[...] = jnp.concatenate(side(factors, 0) + side(factors, 1), axis=0)
     local = jnp.sum(jnp.where(lanes == ep_id, share, 0.0), axis=1, keepdims=True)
-    local = jnp.where(tp_id & 1 == 0, local[:half], local[half:])
+    local = jnp.where(
+        tp_id & 1 == 0,
+        jnp.concatenate(side(local, 0), axis=0),
+        jnp.concatenate(side(local, 1), axis=0),
+    )
     row_count = row_factor.shape[0]
-    local = jnp.concatenate([local] * (row_count // half), axis=0)
-    owned = lax.broadcasted_iota(jnp.int32, row_factor.shape, 0) // half == ep_id
-    row_factor[...] = jnp.where(owned, local, 1.0)
-    row_carry[...] = jnp.where(owned & (tp_id < 2), 1.0, 0.0)
+    local = jnp.concatenate([local] * (row_count // local.shape[0]), axis=0)
+    piece = lax.broadcasted_iota(jnp.int32, row_factor.shape, 0) // portion
+    row_factor[...] = jnp.where(piece // (tp_size // 2) == ep_id, local, 1.0)
+    row_carry[...] = jnp.where(piece == ep_id * (tp_size // 2) + (tp_id >> 1), 1.0, 0.0)
     copies[13].wait()
     recalled = []
     for s in range(seq_rows):
@@ -178,38 +229,74 @@
     mixed = (jax.nn.sigmoid(out_gate) * readout).astype(BF16)
     copies[10].wait()
     head_part = dot(mixed, w_out[...])
-    first = tp_id & 1 == 0
-    own = head_part + jnp.where(tp_id < 2, 1.0, 0.0) * token_rows
-
-    @pl.when(first)
-    def _():
-        sent[...] = head_part[half:].astype(BF16)
-        kept[...] = own[:half]
-
-    @pl.when(jnp.logical_not(first))
-    def _():
-        sent[...] = head_part[:half].astype(BF16)
-        kept[...] = own[half:]
+    for t in range(tp_size):
+
+        @pl.when(tp_id == t)
+        def _():
+            mine = slice(portion * t, portion * (t + 1))
+            kept[...] = head_part[mine] + token_rows[mine]
+            for r in range(1, tp_size):
+                peer = t ^ r
+                theirs = slice(portion * peer, portion * (peer + 1))
+                sents[r - 1][...] = head_part[theirs].astype(BF16)
 
     for write in writes:
         write.wait()
 
 
-def spread_kernel(kept, met, outbound):
-    pair_sum = (kept[...] + met[...].astype(F32)).astype(BF16)
+def spread_kernel(kept, gain, *rest):
+    mets, (residual_out, outbound) = rest[:-2], rest[-2:]
+    residual = kept[...]
+    for met in mets:
+        residual = residual + met[...].astype(F32)
+    residual_out[...] = residual
+    normed = normalize(residual, gain[...]).astype(BF16)
     for n in range(outbound.shape[0]):
-        outbound[n] = pair_sum
-
-
-def load_kernel(*refs):
-    count = len(refs) // 2
-    sems = refs[-1]
-    copies = [
-        pltpu.make_async_copy(refs[n], refs[count + n], sems.at[n]) for n in range(count)
-    ]
-    for copy in copies:
-        copy.start()
-    for copy in copies:
+        outbound[n] = normed
+
+
+def window_kernel(
+    keep_row,
+    fresh,
+    values,
+    memory_hbm,
+    gate_hbm,
+    up_hbm,
+    down_hbm,
+    memory_next,
+    gate,
+    up,
+    down,
+    memory,
+    load_sems,
+    read_sems,
+    write_sems,
+):
+    count = memory.shape[0]
+    reads = [
+        pltpu.make_async_copy(memory_hbm.at[s], memory.at[s], read_sems.at[s])
+        for s in range(count)
+    ]
+    for read in reads:
+        read.start()
+    pairs = ((gate_hbm, gate), (up_hbm, up), (down_hbm, down))
+    loads = [
+        pltpu.make_async_copy(src, dst, load_sems.at[n]) for n, (src, dst) in enumerate(pairs)
+    ]
+    for load in loads:
+        load.start()
+    keep = as_column(keep_row[...])
+    columns = fresh[...].T
+    writes = []
+    for s in range(count):
+        reads[s].wait()
+        memory[s, 0] = (
+            keep[s : s + 1] * memory[s, 0] + columns[:, s : s + 1] * values[s : s + 1, :]
+        )
+        write = pltpu.make_async_copy(memory.at[s], memory_next.at[s], write_sems.at[s])
+        write.start()
+        writes.append(write)
+    for copy in loads + writes:
         copy.wait()
 
 
@@ -217,7 +304,7 @@
     arrived,
     row_factor,
     row_carry,
-    gain,
+    residual,
     gate_a,
     up_a,
     down_a,
@@ -225,19 +312,19 @@
     up_b,
     down_b,
     blocks,
-    residual,
+    gathered,
+    repeated,
 ):
     half, quarter = blocks.shape[1:]
-    rows, width = residual.shape
+    rows, width = gathered.shape
     ep_size = rows // half
-    duo = arrived.shape[0] // ep_size
+    portion = arrived.shape[1]
     tp_size = width // quarter
-    for e in range(ep_size):
-        total = arrived[e * duo].astype(F32)
-        for x in range(1, duo):
-            total = total + arrived[e * duo + x].astype(F32)
-        residual[e * half : (e + 1) * half, :] = total
-    rows_in = normalize(residual[...], gain[...]).astype(BF16)
+    for n in range(arrived.shape[0]):
+        gathered[n * portion : (n + 1) * portion, :] = arrived[n].astype(F32)
+    for n in range(repeated.shape[0] // portion):
+        repeated[n * portion : (n + 1) * portion, :] = residual[...]
+    rows_in = gathered[...].astype(BF16)
 
     def hidden(gate, up):
         both = dot(rows_in, jnp.concatenate([gate[...], up[...]], axis=1))
@@ -246,7 +333,8 @@
 
     hiddens = jnp.concatenate([hidden(gate_a, up_a), hidden(gate_b, up_b)], axis=1)
     part = dot(hiddens, jnp.concatenate([down_a[...], down_b[...]], axis=0))
-    part = row_factor[:, :1] * part + row_carry[:, :1] * residual[...]
+    carried = jnp.concatenate([repeated[...]] * (rows // repeated.shape[0]), axis=0)
+    part = row_factor[:, :1] * part + row_carry[:, :1] * carried
     for e in range(ep_size):
         for t in range(tp_size):
             piece = part[e * half : (e + 1) * half, t * quarter : (t + 1) * quarter]
@@ -256,6 +344,8 @@
 def combine_kernel(returned, factors, output, *, ep_size):
     half = returned.shape[1]
     tp_size = returned.shape[0] // ep_size
+    portion = 2 * half // tp_size
+    totals = []
     for c in range(2):
         rows = slice(c * half, (c + 1) * half)
         total = 0.0
@@ -264,7 +354,11 @@
             for x in range(1, tp_size // 2):
                 value = value + returned[e * tp_size + 2 * x + c].astype(F32)
             total = total + factors[rows, e : e + 1] * value
-        output[rows, :] = total.astype(BF16)
+        totals.append(total)
+    pieces = [
+        totals[t % 2][portion * (t // 2) : portion * (t // 2 + 1)] for t in range(tp_size)
+    ]
+    output[...] = jnp.concatenate(pieces, axis=0).astype(BF16)
 
 
 def shards(
@@ -295,6 +389,7 @@
     quarter = width // tp_size
     half = seq_rows // 2
     duo = tp_size // 2
+    portion = seq_rows // tp_size
     swap = [(t, t ^ 1) for t in range(tp_size)]
     same_side = [
         [e * tp_size + x * 2 + c for e in range(ep_size) for x in range(duo)] for c in range(2)
@@ -324,11 +419,12 @@
         route_weight.T,
     )
     lane_width = -(-ep_size // 128) * 128
-    sent, kept, factors, row_factor, row_carry, norm_next, stab_row, keep, fresh, values = pl.pallas_call(
-        cell_kernel,
+    peers = tp_size - 1
+    results = pl.pallas_call(
+        functools.partial(cell_kernel, tp_size=tp_size),
         out_shape=(
-            shape((half, width), BF16),
-            shape((half, width), F32),
+            *[shape((portion, width), BF16)] * peers,
+            shape((portion, width), F32),
             shape((seq_rows, lane_width), F32),
             shape((ep_size * half, 128), F32),
             shape((ep_size * half, 128), F32),
@@ -339,7 +435,7 @@
             shape((seq_rows, head_size), F32),
         ),
         in_specs=[smem] + [hbm] * len(loads),
-        out_specs=(vmem,) * 5 + (hbm,) * 2 + (vmem,) * 3,
+        out_specs=(vmem,) * (peers + 4) + (hbm,) * 2 + (vmem,) * 3,
         scratch_shapes=[pltpu.VMEM(array.shape, array.dtype) for array in loads]
         + [
             pltpu.VMEM(normalizer.shape, F32),
@@ -353,43 +449,64 @@
         forget_bias,
         *[pltpu.with_memory_space_constraint(array, pltpu.HBM) for array in loads],
     )
+    sents, results = results[:peers], results[peers:]
+    kept, factors, row_factor, row_carry, norm_next, stab_row, *state = results
     weights = (expert_gate[0], expert_up[0], expert_down[0])
-    sent, weights = lax.optimization_barrier((sent, weights))
-    met = lax.ppermute(sent, "tp", swap)
+    sents, weights = lax.optimization_barrier((sents, weights))
+    mets = [
+        lax.ppermute(sents[r - 1], "tp", [(t, t ^ r) for t in range(tp_size)])
+        for r in range(1, tp_size)
+    ]
     mates = [lax.ppermute(weight, "tp", swap) for weight in weights]
-    outbound = pl.pallas_call(
+    residual, outbound = pl.pallas_call(
         spread_kernel,
-        out_shape=shape((ep_size * duo, half, width), BF16),
-        in_specs=[vmem] * 2,
-        out_specs=vmem,
+        out_shape=(
+            shape((portion, width), F32),
+            shape((ep_size * duo, portion, width), BF16),
+        ),
+        in_specs=[vmem] * (peers + 2),
+        out_specs=(vmem, vmem),
         compiler_params=room(8192),
         name="spread",
-    )(kept, met)
+    )(kept, gain_moe.reshape(1, -1), *mets)
     arrived = lax.all_to_all(
         outbound, BOTH, 0, 0, tiled=True, axis_index_groups=same_side
     )
-    memory_next = (
-        keep.reshape(seq_rows, 1, 1, 1) * memory
-        + fresh[:, None, :, None] * values[:, None, None, :]
-    )
-    owned = pl.pallas_call(
-        load_kernel,
-        out_shape=tuple(shape(array.shape, array.dtype) for array in weights),
-        in_specs=[hbm] * 3,
-        out_specs=(vmem,) * 3,
-        scratch_shapes=[pltpu.SemaphoreType.DMA((3,))],
-        compiler_params=room(8192),
-        name="loader",
-    )(*[pltpu.with_memory_space_constraint(array, pltpu.HBM) for array in weights])
+    memory_next, *owned = pl.pallas_call(
+        window_kernel,
+        out_shape=(
+            shape(memory.shape, F32),
+            *[shape(array.shape, array.dtype) for array in weights],
+        ),
+        in_specs=[vmem] * 3 + [hbm] * 4,
+        out_specs=(hbm,) + (vmem,) * 3,
+        scratch_shapes=[
+            pltpu.VMEM(memory.shape, F32),
+            pltpu.SemaphoreType.DMA((3,)),
+            pltpu.SemaphoreType.DMA((seq_rows,)),
+            pltpu.SemaphoreType.DMA((seq_rows,)),
+        ],
+        compiler_params=room(12288),
+        name="keeper",
+    )(
+        *state,
+        *[
+            pltpu.with_memory_space_constraint(array, pltpu.HBM)
+            for array in (memory, *weights)
+        ],
+    )
     blocks = pl.pallas_call(
         expert_kernel,
         out_shape=shape((ep_size * tp_size, half, quarter), BF16),
         in_specs=[vmem] * 10,
         out_specs=vmem,
-        scratch_shapes=[pltpu.VMEM((ep_size * half, width), F32)],
+        scratch_shapes=[
+            pltpu.VMEM((ep_size * half, width), F32),
+            pltpu.VMEM((8, width), F32),
+        ],
         compiler_params=room(24576),
         name="experts",
-    )(arrived, row_factor, row_carry, gain_moe.reshape(1, -1), *owned, *mates)
+    )(arrived, row_factor, row_carry, residual, *owned, *mates)
     returned = lax.all_to_all(blocks, BOTH, 0, 0, tiled=True)
     output = pl.pallas_call(
         functools.partial(combine_kernel, ep_size=ep_size),

time: 41.5 us -> 40.7 us (0.981)
  blocking collectives: 0 us -> 10.1 us
  waiting for transfers between devices: 16.4 us -> 6.37 us
  other arithmetic: 3.27 us -> 0 us
  starting transfers between devices: 11.9 us -> 13.8 us
  Pallas kernels: 8.23 us -> 8.91 us
    all_to_all x0 -> x1, blocking collectives: none -> 10.1 us  [shards(): returned = lax.all_to_all(blocks, BOTH, 0, 0, tiled=True)]
    ppermute x1 -> x3, starting transfers between devices: 0.08 us -> 5.33 us  [shards(): lax.ppermute(sents[r - 1], 'tp', [(t, t ^ r) for t in range(tp_size)])]
    all_to_all x1 -> x0, waiting for transfers between devices: 4.93 us -> none  [shards(): returned = lax.all_to_all(blocks, BOTH, 0, 0, tiled=True)]
    all_to_all x1, waiting for transfers between devices: 8.78 us -> 4.99 us  [shards(): lax.all_to_all(outbound, BOTH, 0, 0, tiled=True, axis_index_groups=same_s...]
    add x1 -> x0, other arithmetic: 3.27 us -> none  [shards(): keep.reshape(seq_rows, 1, 1, 1) * memory]
    all_to_all x1 -> x0, starting transfers between devices: 2.57 us -> none  [shards(): returned = lax.all_to_all(blocks, BOTH, 0, 0, tiled=True)]
    pallas_call x3, Pallas kernels: 5.96 us -> 7.5 us  [the longest x1 3.84 us: shards(): pl.pallas_call(functools.partial(cell_kernel, tp_size=tp_size), out_shape...]
    ppermute x1 -> x3, waiting for transfers between devices: 2.68 us -> 1.37 us  [shards(): lax.ppermute(sents[r - 1], 'tp', [(t, t ^ r) for t in range(tp_size)])]
  transfers between devices with their start and end apart: 6 -> 7, of which waited for: 3 -> 2; matrix products, arithmetic and copies ran while one was open for 8% -> 0% of each run, Pallas kernels for 5% -> 9%
where the time goes in v4:
time: 40.7 us; the launch traced here: 40.5 us
  starting transfers between devices  13.8 us (34%)
  blocking collectives  10.1 us (25%)
  Pallas kernels  8.91 us (22%)
  waiting for transfers between devices  6.37 us (16%)
  between operations  1.33 us (3%)
    all_to_all x1, blocking collectives, shards(): returned = lax.all_to_all(blocks, BOTH, 0, 0, tiled=True)  10.1 us
    all_to_all x1, starting transfers between devices, shards(): lax.all_to_all(outbound, BOTH, 0, 0, tiled=True, axis_index_groups=same_s...  7.34 us
    ppermute x3, starting transfers between devices, shards(): lax.ppermute(sents[r - 1], 'tp', [(t, t ^ r) for t in range(tp_size)])  5.33 us
    all_to_all x1, waiting for transfers between devices, shards(): lax.all_to_all(outbound, BOTH, 0, 0, tiled=True, axis_index_groups=same_s...  4.99 us
    pallas_call x1, Pallas kernels, shards(): pl.pallas_call(functools.partial(cell_kernel, tp_size=tp_size), out_shape...  3.84 us
    pallas_call x1, Pallas kernels, shards(): pl.pallas_call(window_kernel, out_shape=(shape(memory.shape, F32), *[shap...  2.8 us
    ppermute x3, waiting for transfers between devices, shards(): lax.ppermute(sents[r - 1], 'tp', [(t, t ^ r) for t in range(tp_size)])  1.37 us
    ppermute x3, starting transfers between devices, shards(): mates = [lax.ppermute(weight, 'tp', swap) for weight in weights]  1.08 us
  transfers between devices with their start and end apart: 7, of which 2 were waited for; matrix products, arithmetic and copies ran while one was open for 0% of the time, Pallas kernels for 9%

profile of v4, /device:TPU:0, one launch (start us, length us, event | category | flops | bytes accessed | tf_op | source)
XLA Modules:
  0.0 40.5 jit_solution(6287487776502485930)
XLA Ops:
  1.3 0.0 copy-start
  1.3 3.8 %cell.1 = (bf16[2,2048]{1,0:T(2,128)(2,1)S(1)}, bf16[2,2048]{1,0:T(2,128)(2,1)S(1)}, bf16[2,2048]{1,0:T(2,128)(2,1)S(1)}, f32[2,2048]{1,0:T(2,128)S(1)}, f32[8,1...) custom-call(f32[1]{0:T(128)S(6)} %copy.23.bias, ...), custom_call_target="tpu_custom_call" | custom-call | tf_op jit(solution)/shard_map/cell/pallas_call | solution.py:423
  5.1 0.6 %collective-permute-start.3 = (bf16[2048,128]{1,0:T(8,128)(2,1)}, bf16[2048,128]{1,0:T(8,128)(2,1)S(1)}, u32[]{:S(2)}, u32[]{:S(2)}) collective-permute-start(bf16[2048,128]{1,0:T(8,128)(2,1)} %bitcast.7.gate_hbm), channel_id=1, source_target_pairs={{0,1},{1,0},{2,3},{3,2},{4,5},{5,4},{6,7},{7,6},{8,9},{9,8},{10,11... | collective-permute-start | bytes 1572872 | tf_op jit(solution)/shard_map/ppermute | solution.py:460
  5.7 0.1 collective-permute-start.4
  5.8 0.4 %collective-permute-start.5 = (bf16[128,2048]{1,0:T(8,128)(2,1)}, bf16[128,2048]{1,0:T(8,128)(2,1)S(1)}, u32[]{:S(2)}, u32[]{:S(2)}) collective-permute-start(bf16[128,2048]{1,0:T(8,128)(2,1)} %bitcast.9.down_hbm), channel_id=1, source_target_pairs={{0,1},{1,0},{2,3},{3,2},{4,5},{5,4},{6,7},{7,6},{8,9},{9,8},{10,11... | collective-permute-start | bytes 1572872 | tf_op jit(solution)/shard_map/ppermute | solution.py:460
  6.2 0.1 collective-permute-start
  6.3 2.9 %collective-permute-start.1 = (bf16[2,2048]{1,0:T(2,128)(2,1)S(1)}, bf16[2,2048]{1,0:T(2,128)(2,1)S(1)}, u32[]{:S(2)}, u32[]{:S(2)}) collective-permute-start(bf16[2,2048]{1,0:T(2,128)(2,1)S(1)} %get-tuple-element.33), channel_id=1, source_target_pairs={{0,2},{1,3},{2,0},{3,1},{4,6},{5,7},{6,4},{7,5},{8,10},{9,11},{10,... | collective-permute-start | bytes 24584 | tf_op jit(solution)/shard_map/ppermute | solution.py:457
  9.2 0.0 collective-permute-done.rest_0_
  9.2 2.3 %collective-permute-start.2 = (bf16[2,2048]{1,0:T(2,128)(2,1)S(1)}, bf16[2,2048]{1,0:T(2,128)(2,1)S(1)}, u32[]{:S(2)}, u32[]{:S(2)}) collective-permute-start(bf16[2,2048]{1,0:T(2,128)(2,1)S(1)} %get-tuple-element.34), channel_id=1, source_target_pairs={{0,3},{1,2},{2,1},{3,0},{4,7},{5,6},{6,5},{7,4},{8,11},{9,10},{10,... | collective-permute-start | bytes 24584 | tf_op jit(solution)/shard_map/ppermute | solution.py:457
  11.6 0.0 collective-permute-done.1.rest_1_
  11.6 1.4 %collective-permute-done.2.rest_2_ = bf16[2,2048]{1,0:T(2,128)(2,1)S(1)} collective-permute-done((bf16[2,2048]{1,0:T(2,128)(2,1)S(1)}, bf16[2,2048]{1,0:T(2,128)(2,1)S(1)}, u32[]{:S(2)}, u32[]{:S(2)}) %collective-permute-start.2) | collective-permute-done | bytes 8224 | tf_op jit(solution)/shard_map/ppermute | solution.py:457
  12.9 0.0 copy-done
  12.9 0.9 %spread.1 = (f32[2,2048]{1,0:T(2,128)S(1)}, bf16[16,2,2048]{2,1,0:T(2,128)(2,1)}) custom-call(f32[2,2048]{1,0:T(2,128)S(1)} %get-tuple-element.28.kept, f32[1,2048]{1,0:T(1,128)S(1)} %bitcast.11, bf16[2,2048]{1,0:T(2,128)(2,1)S(1)} %collective-permute-done.rest_0_, bf16[2,2048]{1,0:T(2,128)(2,1)S(1)} %collective-permute-done.1.rest_1_, ...), custom_call_target="tpu_custom_call" | custom-call | tf_op jit(solution)/shard_map/spread/pallas_call | solution.py:461
  13.8 7.3 %all-to-all-start = ((bf16[16,2,2048]{2,1,0:T(2,128)(2,1)}), bf16[16,2,2048]{2,1,0:T(2,128)(2,1)S(1)}, u32[]{:S(2)}, u32[]{:S(2)}) async-start(bf16[16,2,2048]{2,1,0:T(2,128)(2,1)} %get-tuple-element.35), calls=%async_computation | async-start | bytes 262144 | tf_op jit(solution)/shard_map/all_to_all | solution.py:472
  21.1 2.8 %keeper.1 = (f32[8,1,256,256]{3,2,1,0:T(8,128)}, bf16[2048,128]{1,0:T(8,128)(2,1)S(1)}, bf16[2048,128]{1,0:T(8,128)(2,1)S(1)}, bf16[128,2048]{1,0:T(8,128)(2,1)S(1)}) custom-call(f32[1,8]{1,0:T(1,128)S(1)} %get-tuple-element.39.keep_row, f32[8,256]{1,0:T(8,128)S(1)} %get-tuple-element.40.fresh, f32[8,256]{1,0:T(8,128)S(1)} %get-tuple-element.41.values, ...), custom_call_target="tpu_custom_call" | custom-call | tf_op jit(solution)/shard_map/keeper/pallas_call | solution.py:475
  23.9 5.0 %all-to-all-done.arrived = bf16[16,2,2048]{2,1,0:T(2,128)(2,1)S(1)} async-done(((bf16[16,2,2048]{2,1,0:T(2,128)(2,1)}), bf16[16,2,2048]{2,1,0:T(2,128)(2,1)S(1)}, u32[]{:S(2)}, u32[]{:S(2)}) %all-to-all-start) | async-done | bytes 131104 | tf_op jit(solution)/shard_map/all_to_all | solution.py:472
  28.9 0.0 collective-permute-done.3.gate_b
  28.9 0.0 collective-permute-done.4.up_b
  28.9 0.0 collective-permute-done.5.down_b
  28.9 0.7 %experts.1 = bf16[32,4,512]{2,1,0:T(4,128)(2,1)S(1)} custom-call(bf16[16,2,2048]{2,1,0:T(2,128)(2,1)S(1)} %all-to-all-done.arrived, f32[32,128]{1,0:T(8,128)S(1)} %get-tuple-element.36.row_factor, f32[32,128]{1,0:T(8,128)S(1)} %get-tuple-element.37.row_carry, f32[2,2048]{1,0:T(2,128)S(1)} %get-tuple-element.38.residual, ...), custom_call_target="tpu_custom_call" | custom-call | tf_op jit(solution)/shard_map/experts/pallas_call | solution.py:498
  29.7 10.1 %all_to_all.10.returned = bf16[32,4,512]{2,1,0:T(4,128)(2,1)S(1)} all-to-all(bf16[32,4,512]{2,1,0:T(4,128)(2,1)S(1)} %experts.1), channel_id=1, replica_groups=mesh['ep'=8,'tp'=4] {'ep','tp'}, dimensions={0} | all-to-all | bytes 262144 | tf_op jit(solution)/shard_map/all_to_all | solution.py:510
  39.8 0.7 %combine.1 = bf16[8,512]{1,0:T(8,128)(2,1)} custom-call(bf16[32,4,512]{2,1,0:T(4,128)(2,1)S(1)} %all_to_all.10.returned, f32[8,128]{1,0:T(8,128)S(1)} %get-tuple-element.48.factors), custom_call_target="tpu_custom_call" | custom-call | tf_op jit(solution)/shard_map/combine/pallas_call | solution.py:511
Async XLA Ops:
  1.3 11.6 %copy-start = (f32[2048]{0:T(1024)S(1)}, f32[2048]{0:T(1024)}, u32[]{:S(2)}) copy-start(f32[2048]{0:T(1024)} %param.29) | copy-start | bytes 24580
  5.1 23.8 %collective-permute-start.3 = (bf16[2048,128]{1,0:T(8,128)(2,1)}, bf16[2048,128]{1,0:T(8,128)(2,1)S(1)}, u32[]{:S(2)}, u32[]{:S(2)}) collective-permute-start(bf16[2048,128]{1,0:T(8,128)(2,1)} %bitcast.7.gate_hbm), channel_id=1, source_target_pairs={{0,1},{1,0},{2,3},{3,2},{4,5},{5,4},{6,7},{7,6},{8,9},{9,8},{10,11... | collective-permute-start | bytes 1572872 | tf_op jit(solution)/shard_map/ppermute | solution.py:460
  5.7 23.2 %collective-permute-start.4 = (bf16[2048,128]{1,0:T(8,128)(2,1)}, bf16[2048,128]{1,0:T(8,128)(2,1)S(1)}, u32[]{:S(2)}, u32[]{:S(2)}) collective-permute-start(bf16[2048,128]{1,0:T(8,128)(2,1)} %bitcast.8.up_hbm), channel_id=1, source_target_pairs={{0,1},{1,0},{2,3},{3,2},{4,5},{5,4},{6,7},{7,6},{8,9},{9,8},{10,11... | collective-permute-start | bytes 1572872 | tf_op jit(solution)/shard_map/ppermute | solution.py:460
  5.8 23.1 %collective-permute-start.5 = (bf16[128,2048]{1,0:T(8,128)(2,1)}, bf16[128,2048]{1,0:T(8,128)(2,1)S(1)}, u32[]{:S(2)}, u32[]{:S(2)}) collective-permute-start(bf16[128,2048]{1,0:T(8,128)(2,1)} %bitcast.9.down_hbm), channel_id=1, source_target_pairs={{0,1},{1,0},{2,3},{3,2},{4,5},{5,4},{6,7},{7,6},{8,9},{9,8},{10,11... | collective-permute-start | bytes 1572872 | tf_op jit(solution)/shard_map/ppermute | solution.py:460
  6.2 3.0 %collective-permute-start = (bf16[2,2048]{1,0:T(2,128)(2,1)S(1)}, bf16[2,2048]{1,0:T(2,128)(2,1)S(1)}, u32[]{:S(2)}, u32[]{:S(2)}) collective-permute-start(bf16[2,2048]{1,0:T(2,128)(2,1)S(1)} %get-tuple-element.32), channel_id=1, source_target_pairs={{0,1},{1,0},{2,3},{3,2},{4,5},{5,4},{6,7},{7,6},{8,9},{9,8},{10,11... | collective-permute-start | bytes 24584 | tf_op jit(solution)/shard_map/ppermute | solution.py:457
  6.3 5.3 %collective-permute-start.1 = (bf16[2,2048]{1,0:T(2,128)(2,1)S(1)}, bf16[2,2048]{1,0:T(2,128)(2,1)S(1)}, u32[]{:S(2)}, u32[]{:S(2)}) collective-permute-start(bf16[2,2048]{1,0:T(2,128)(2,1)S(1)} %get-tuple-element.33), channel_id=1, source_target_pairs={{0,2},{1,3},{2,0},{3,1},{4,6},{5,7},{6,4},{7,5},{8,10},{9,11},{10,... | collective-permute-start | bytes 24584 | tf_op jit(solution)/shard_map/ppermute | solution.py:457
  9.2 3.7 %collective-permute-start.2 = (bf16[2,2048]{1,0:T(2,128)(2,1)S(1)}, bf16[2,2048]{1,0:T(2,128)(2,1)S(1)}, u32[]{:S(2)}, u32[]{:S(2)}) collective-permute-start(bf16[2,2048]{1,0:T(2,128)(2,1)S(1)} %get-tuple-element.34), channel_id=1, source_target_pairs={{0,3},{1,2},{2,1},{3,0},{4,7},{5,6},{6,5},{7,4},{8,11},{9,10},{10,... | collective-permute-start | bytes 24584 | tf_op jit(solution)/shard_map/ppermute | solution.py:457
  13.8 15.1 %all-to-all-start = ((bf16[16,2,2048]{2,1,0:T(2,128)(2,1)}), bf16[16,2,2048]{2,1,0:T(2,128)(2,1)S(1)}, u32[]{:S(2)}, u32[]{:S(2)}) async-start(bf16[16,2,2048]{2,1,0:T(2,128)(2,1)} %get-tuple-element.35), calls=%async_computation | async-start | bytes 262144 | tf_op jit(solution)/shard_map/all_to_all | solution.py:472

commit v5 on v4

--- a/solution.py
+++ b/solution.py
@@ -105,9 +105,7 @@
     row_carry,
     norm_hbm,
     stabilizer_next_hbm,
-    keep_out,
-    fresh_out,
-    values_out,
+    memory_next,
     tokens,
     gain,
     w_in,
@@ -169,7 +167,6 @@
     keep = jnp.exp(shifted - stab)
     admit = jnp.exp(gate_in - stab)
     stabilizer_next[...] = as_row(stab)
-    keep_out[...] = as_row(keep)
     writes = [
         pltpu.make_async_copy(stabilizer_next, stabilizer_next_hbm, write_sems.at[0]),
         pltpu.make_async_copy(norm_next, norm_hbm, write_sems.at[1]),
@@ -188,8 +185,7 @@
     grown = keep * normalizer[...].reshape(seq_rows, head_size) + fresh
     norm_next[...] = grown.reshape(norm_next.shape)
     writes[1].start()
-    fresh_out[...] = fresh
-    values_out[...] = values
+    fresh_columns = fresh.T
     match = jnp.sum(queries * fresh, axis=1, keepdims=True)
     divisor = jnp.maximum(
         jnp.abs(jnp.sum(queries * grown, axis=1, keepdims=True)), jnp.exp(-stab)
@@ -222,7 +218,14 @@
     copies[13].wait()
     recalled = []
     for s in range(seq_rows):
-        recalled.append(jnp.sum(columns[:, s : s + 1] * memory[s, 0], axis=0, keepdims=True))
+        matrix = memory[s, 0]
+        recalled.append(jnp.sum(columns[:, s : s + 1] * matrix, axis=0, keepdims=True))
+        memory[s, 0] = (
+            keep[s : s + 1] * matrix + fresh_columns[:, s : s + 1] * values[s : s + 1]
+        )
+        write = pltpu.make_async_copy(memory.at[s], memory_next.at[s], write_sems.at[2 + s])
+        write.start()
+        writes.append(write)
     old = jnp.concatenate(recalled, axis=0)
     readout = (keep * old + match * values) / divisor
     out_gate = project(9, wo)
@@ -253,51 +256,6 @@
     normed = normalize(residual, gain[...]).astype(BF16)
     for n in range(outbound.shape[0]):
         outbound[n] = normed
-
-
-def window_kernel(
-    keep_row,
-    fresh,
-    values,
-    memory_hbm,
-    gate_hbm,
-    up_hbm,
-    down_hbm,
-    memory_next,
-    gate,
-    up,
-    down,
-    memory,
-    load_sems,
-    read_sems,
-    write_sems,
-):
-    count = memory.shape[0]
-    reads = [
-        pltpu.make_async_copy(memory_hbm.at[s], memory.at[s], read_sems.at[s])
-        for s in range(count)
-    ]
-    for read in reads:
-        read.start()
-    pairs = ((gate_hbm, gate), (up_hbm, up), (down_hbm, down))
-    loads = [
-        pltpu.make_async_copy(src, dst, load_sems.at[n]) for n, (src, dst) in enumerate(pairs)
-    ]
-    for load in loads:
-        load.start()
-    keep = as_column(keep_row[...])
-    columns = fresh[...].T
-    writes = []
-    for s in range(count):
-        reads[s].wait()
-        memory[s, 0] = (
-            keep[s : s + 1] * memory[s, 0] + columns[:, s : s + 1] * values[s : s + 1, :]
-        )
-        write = pltpu.make_async_copy(memory.at[s], memory_next.at[s], write_sems.at[s])
-        write.start()
-        writes.append(write)
-    for copy in loads + writes:
-        copy.wait()
 
 
 def expert_kernel(
@@ -385,7 +343,6 @@
     ep_size = lax.axis_size("ep")
     tp_size = lax.axis_size("tp")
     seq_rows, width = tokens.shape
-    head_size = memory.shape[2]
     quarter = width // tp_size
     half = seq_rows // 2
     duo = tp_size // 2
@@ -430,18 +387,16 @@
             shape((ep_size * half, 128), F32),
             shape(normalizer.shape, F32),
             shape((1, seq_rows), F32),
-            shape((1, seq_rows), F32),
-            shape((seq_rows, head_size), F32),
-            shape((seq_rows, head_size), F32),
+            shape(memory.shape, F32),
         ),
         in_specs=[smem] + [hbm] * len(loads),
-        out_specs=(vmem,) * (peers + 4) + (hbm,) * 2 + (vmem,) * 3,
+        out_specs=(vmem,) * (peers + 4) + (hbm,) * 3,
         scratch_shapes=[pltpu.VMEM(array.shape, array.dtype) for array in loads]
         + [
             pltpu.VMEM(normalizer.shape, F32),
             pltpu.VMEM((1, seq_rows), F32),
             pltpu.SemaphoreType.DMA((len(loads),)),
-            pltpu.SemaphoreType.DMA((2,)),
+            pltpu.SemaphoreType.DMA((2 + seq_rows,)),
         ],
         compiler_params=room(20480),
         name="cell",
@@ -450,12 +405,12 @@
         *[pltpu.with_memory_space_constraint(array, pltpu.HBM) for array in loads],
     )
     sents, results = results[:peers], results[peers:]
-    kept, factors, row_factor, row_carry, norm_next, stab_row, *state = results
+    kept, factors, row_factor, row_carry, norm_next, stab_row, memory_next = results
     weights = (expert_gate[0], expert_up[0], expert_down[0])
     sents, weights = lax.optimization_barrier((sents, weights))
     mets = [
         lax.ppermute(sents[r - 1], "tp", [(t, t ^ r) for t in range(tp_size)])
-        for r in range(1, tp_size)
+        for r in range(tp_size - 1, 0, -1)
     ]
     mates = [lax.ppermute(weight, "tp", swap) for weight in weights]
     residual, outbound = pl.pallas_call(
@@ -472,29 +427,6 @@
     arrived = lax.all_to_all(
         outbound, BOTH, 0, 0, tiled=True, axis_index_groups=same_side
     )
-    memory_next, *owned = pl.pallas_call(
-        window_kernel,
-        out_shape=(
-            shape(memory.shape, F32),
-            *[shape(array.shape, array.dtype) for array in weights],
-        ),
-        in_specs=[vmem] * 3 + [hbm] * 4,
-        out_specs=(hbm,) + (vmem,) * 3,
-        scratch_shapes=[
-            pltpu.VMEM(memory.shape, F32),
-            pltpu.SemaphoreType.DMA((3,)),
-            pltpu.SemaphoreType.DMA((seq_rows,)),
-            pltpu.SemaphoreType.DMA((seq_rows,)),
-        ],
-        compiler_params=room(12288),
-        name="keeper",
-    )(
-        *state,
-        *[
-            pltpu.with_memory_space_constraint(array, pltpu.HBM)
-            for array in (memory, *weights)
-        ],
-    )
     blocks = pl.pallas_call(
         expert_kernel,
         out_shape=shape((ep_size * tp_size, half, quarter), BF16),
@@ -506,7 +438,7 @@
         ],
         compiler_params=room(24576),
         name="experts",
-    )(arrived, row_factor, row_carry, residual, *owned, *mates)
+    )(arrived, row_factor, row_carry, residual, *weights, *mates)
     returned = lax.all_to_all(blocks, BOTH, 0, 0, tiled=True)
     output = pl.pallas_call(
         functools.partial(combine_kernel, ep_size=ep_size),

time: 40.7 us -> 38.8 us (0.953)
  blocking collectives: 10.1 us -> 23.9 us
  starting transfers between devices: 13.8 us -> 3.74 us
  Pallas kernels: 8.91 us -> 6.03 us
  waiting for transfers between devices: 6.37 us -> 3.58 us
    all_to_all x0 -> x1, blocking collectives: none -> 13.8 us  [shards(): lax.all_to_all(outbound, BOTH, 0, 0, tiled=True, axis_index_groups=same_s...]
    all_to_all x1 -> x0, starting transfers between devices: 7.34 us -> none  [shards(): lax.all_to_all(outbound, BOTH, 0, 0, tiled=True, axis_index_groups=same_s...]
    all_to_all x1 -> x0, waiting for transfers between devices: 4.99 us -> none  [shards(): lax.all_to_all(outbound, BOTH, 0, 0, tiled=True, axis_index_groups=same_s...]
    pallas_call x1 -> x0, Pallas kernels: 2.8 us -> none  [shards(): pl.pallas_call(window_kernel, out_shape=(shape(memory.shape, F32), *[shap...]
    ppermute x3, starting transfers between devices: 5.33 us -> 2.67 us  [shards(): lax.ppermute(sents[r - 1], 'tp', [(t, t ^ r) for t in range(tp_size)])]
    ppermute x3, waiting for transfers between devices: 1.37 us -> 3.57 us  [shards(): lax.ppermute(sents[r - 1], 'tp', [(t, t ^ r) for t in range(tp_size)])]
    pallas_call x1, Pallas kernels: 0.86 us -> 0.22 us  [shards(): pl.pallas_call(spread_kernel, out_shape=(shape((portion, width), F32), sh...]
    pallas_call x1, Pallas kernels: 3.84 us -> 4.38 us  [shards(): pl.pallas_call(functools.partial(cell_kernel, tp_size=tp_size), out_shape...]
  transfers between devices with their start and end apart: 7 -> 6, of which waited for: 2 -> 2; matrix products, arithmetic and copies ran while one was open for 0% -> 0% of each run, Pallas kernels for 9% -> 1%
where the time goes in v5:
time: 38.8 us; the launch traced here: 38.6 us
  blocking collectives  23.9 us (62%)
  Pallas kernels  6.03 us (16%)
  starting transfers between devices  3.74 us (10%)
  waiting for transfers between devices  3.58 us (9%)
  between operations  1.36 us (4%)
    all_to_all x1, blocking collectives, shards(): lax.all_to_all(outbound, BOTH, 0, 0, tiled=True, axis_index_groups=same_s...  13.8 us
    all_to_all x1, blocking collectives, shards(): returned = lax.all_to_all(blocks, BOTH, 0, 0, tiled=True)  10.2 us
    pallas_call x1, Pallas kernels, shards(): pl.pallas_call(functools.partial(cell_kernel, tp_size=tp_size), out_shape...  4.38 us
    ppermute x3, waiting for transfers between devices, shards(): lax.ppermute(sents[r - 1], 'tp', [(t, t ^ r) for t in range(tp_size)])  3.57 us
    ppermute x3, starting transfers between devices, shards(): lax.ppermute(sents[r - 1], 'tp', [(t, t ^ r) for t in range(tp_size)])  2.67 us
    ppermute x3, starting transfers between devices, shards(): mates = [lax.ppermute(weight, 'tp', swap) for weight in weights]  1.07 us
  transfers between devices with their start and end apart: 6, of which 2 were waited for; matrix products, arithmetic and copies ran while one was open for 0% of the time, Pallas kernels for 1%

profile of v5, /device:TPU:0, one launch (start us, length us, event | category | flops | bytes accessed | tf_op | source)
XLA Modules:
  0.0 38.6 jit_solution(8627694905076391427)
XLA Ops:
  1.3 0.0 copy-start
  1.3 0.0 copy-start.1
  1.3 0.0 copy-start.2
  1.3 0.0 copy-start.3
  1.3 4.4 %cell.1 = (bf16[2,2048]{1,0:T(2,128)(2,1)S(1)}, bf16[2,2048]{1,0:T(2,128)(2,1)S(1)}, bf16[2,2048]{1,0:T(2,128)(2,1)S(1)}, f32[2,2048]{1,0:T(2,128)S(1)}, f32[8,1...) custom-call(f32[1]{0:T(128)S(6)} %copy.23.bias, ...), custom_call_target="tpu_custom_call" | custom-call | tf_op jit(solution)/shard_map/cell/pallas_call | solution.py:380
  5.7 0.0 copy-done
  5.7 0.6 %collective-permute-start.3 = (bf16[2048,128]{1,0:T(8,128)(2,1)S(1)}, bf16[2048,128]{1,0:T(8,128)(2,1)S(1)}, u32[]{:S(2)}, u32[]{:S(2)}) collective-permute-start(bf16[2048,128]{1,0:T(8,128)(2,1)S(1)} %bitcast.11), channel_id=1, source_target_pairs={{0,1},{1,0},{2,3},{3,2},{4,5},{5,4},{6,7},{7,6},{8,9},{9,8},{10,11... | collective-permute-start | bytes 1572872 | tf_op jit(solution)/shard_map/ppermute | solution.py:415
  6.3 0.0 copy-done.1
  6.3 0.1 collective-permute-start.4
  6.4 0.0 copy-done.2
  6.4 0.4 %collective-permute-start.5 = (bf16[128,2048]{1,0:T(8,128)(2,1)S(1)}, bf16[128,2048]{1,0:T(8,128)(2,1)S(1)}, u32[]{:S(2)}, u32[]{:S(2)}) collective-permute-start(bf16[128,2048]{1,0:T(8,128)(2,1)S(1)} %bitcast.15), channel_id=1, source_target_pairs={{0,1},{1,0},{2,3},{3,2},{4,5},{5,4},{6,7},{7,6},{8,9},{9,8},{10,11... | collective-permute-start | bytes 1572872 | tf_op jit(solution)/shard_map/ppermute | solution.py:415
  6.8 2.6 %collective-permute-start = (bf16[2,2048]{1,0:T(2,128)(2,1)S(1)}, bf16[2,2048]{1,0:T(2,128)(2,1)S(1)}, u32[]{:S(2)}, u32[]{:S(2)}) collective-permute-start(bf16[2,2048]{1,0:T(2,128)(2,1)S(1)} %get-tuple-element.26), channel_id=1, source_target_pairs={{0,3},{1,2},{2,1},{3,0},{4,7},{5,6},{6,5},{7,4},{8,11},{9,10},{10,... | collective-permute-start | bytes 24584 | tf_op jit(solution)/shard_map/ppermute | solution.py:412
  9.4 0.0 collective-permute-start.1
  9.4 1.4 %collective-permute-done.rest_0_ = bf16[2,2048]{1,0:T(2,128)(2,1)S(1)} collective-permute-done((bf16[2,2048]{1,0:T(2,128)(2,1)S(1)}, bf16[2,2048]{1,0:T(2,128)(2,1)S(1)}, u32[]{:S(2)}, u32[]{:S(2)}) %collective-permute-start) | collective-permute-done | bytes 8224 | tf_op jit(solution)/shard_map/ppermute | solution.py:412
  10.8 0.1 collective-permute-start.2
  10.8 2.2 %collective-permute-done.1.rest_1_ = bf16[2,2048]{1,0:T(2,128)(2,1)S(1)} collective-permute-done((bf16[2,2048]{1,0:T(2,128)(2,1)S(1)}, bf16[2,2048]{1,0:T(2,128)(2,1)S(1)}, u32[]{:S(2)}, u32[]{:S(2)}) %collective-permute-start.1) | collective-permute-done | bytes 8224 | tf_op jit(solution)/shard_map/ppermute | solution.py:412
  13.0 0.0 collective-permute-done.2.rest_2_
  13.0 0.0 copy-done.3
  13.0 0.2 spread.1
  13.3 13.8 %all_to_all.10.arrived = bf16[16,2,2048]{2,1,0:T(2,128)(2,1)S(1)} all-to-all(bf16[16,2,2048]{2,1,0:T(2,128)(2,1)S(1)} %get-tuple-element.29), channel_id=1, replica_groups={{0,2,4,6,8,10,12,14,16,18,20,22,24,26,28,30},{1,3,5,7,9,11,13,15,17,19,..., dimensions={0} | all-to-all | bytes 262144 | tf_op jit(solution)/shard_map/all_to_all | solution.py:427
  27.0 0.0 collective-permute-done.3.gate_b
  27.0 0.0 collective-permute-done.4.up_b
  27.0 0.0 collective-permute-done.5.down_b
  27.1 0.7 %experts.1 = bf16[32,4,512]{2,1,0:T(4,128)(2,1)S(1)} custom-call(bf16[16,2,2048]{2,1,0:T(2,128)(2,1)S(1)} %all_to_all.10.arrived, f32[32,128]{1,0:T(8,128)S(1)} %get-tuple-element.30.row_factor, f32[32,128]{1,0:T(8,128)S(1)} %get-tuple-element.31.row_carry, f32[2,2048]{1,0:T(2,128)S(1)} %get-tuple-element.32.residual, bf16[2048,128]{1,0:T(8,128)(2,1)S(1)} %bitcast.12, ...), custom_call_target="tpu_custom_call" | custom-call | tf_op jit(solution)/shard_map/experts/pallas_call | solution.py:430
  27.8 10.2 %all_to_all.11.returned = bf16[32,4,512]{2,1,0:T(4,128)(2,1)S(1)} all-to-all(bf16[32,4,512]{2,1,0:T(4,128)(2,1)S(1)} %experts.1), channel_id=1, replica_groups=mesh['ep'=8,'tp'=4] {'ep','tp'}, dimensions={0} | all-to-all | bytes 262144 | tf_op jit(solution)/shard_map/all_to_all | solution.py:442
  37.9 0.7 %combine.1 = bf16[8,512]{1,0:T(8,128)(2,1)} custom-call(bf16[32,4,512]{2,1,0:T(4,128)(2,1)S(1)} %all_to_all.11.returned, f32[8,128]{1,0:T(8,128)S(1)} %get-tuple-element.36.factors), custom_call_target="tpu_custom_call" | custom-call | tf_op jit(solution)/shard_map/combine/pallas_call | solution.py:443
Async XLA Ops:
  1.3 4.4 %copy-start = (bf16[1,2048,128]{2,1,0:T(8,128)(2,1)S(1)}, bf16[1,2048,128]{2,1,0:T(8,128)(2,1)}, u32[]{:S(2)}) copy-start(bf16[1,2048,128]{2,1,0:T(8,128)(2,1)} %param.33) | copy-start | bytes 1572868
  1.3 5.0 %copy-start.1 = (bf16[1,2048,128]{2,1,0:T(8,128)(2,1)S(1)}, bf16[1,2048,128]{2,1,0:T(8,128)(2,1)}, u32[]{:S(2)}) copy-start(bf16[1,2048,128]{2,1,0:T(8,128)(2,1)} %param.34) | copy-start | bytes 1572868
  1.3 5.1 %copy-start.2 = (bf16[1,128,2048]{2,1,0:T(8,128)(2,1)S(1)}, bf16[1,128,2048]{2,1,0:T(8,128)(2,1)}, u32[]{:S(2)}) copy-start(bf16[1,128,2048]{2,1,0:T(8,128)(2,1)} %param.35) | copy-start | bytes 1572868
  1.3 11.7 %copy-start.3 = (f32[2048]{0:T(1024)S(1)}, f32[2048]{0:T(1024)}, u32[]{:S(2)}) copy-start(f32[2048]{0:T(1024)} %param.29) | copy-start | bytes 24580
  5.7 21.3 %collective-permute-start.3 = (bf16[2048,128]{1,0:T(8,128)(2,1)S(1)}, bf16[2048,128]{1,0:T(8,128)(2,1)S(1)}, u32[]{:S(2)}, u32[]{:S(2)}) collective-permute-start(bf16[2048,128]{1,0:T(8,128)(2,1)S(1)} %bitcast.11), channel_id=1, source_target_pairs={{0,1},{1,0},{2,3},{3,2},{4,5},{5,4},{6,7},{7,6},{8,9},{9,8},{10,11... | collective-permute-start | bytes 1572872 | tf_op jit(solution)/shard_map/ppermute | solution.py:415
  6.3 20.8 %collective-permute-start.4 = (bf16[2048,128]{1,0:T(8,128)(2,1)S(1)}, bf16[2048,128]{1,0:T(8,128)(2,1)S(1)}, u32[]{:S(2)}, u32[]{:S(2)}) collective-permute-start(bf16[2048,128]{1,0:T(8,128)(2,1)S(1)} %bitcast.13), channel_id=1, source_target_pairs={{0,1},{1,0},{2,3},{3,2},{4,5},{5,4},{6,7},{7,6},{8,9},{9,8},{10,11... | collective-permute-start | bytes 1572872 | tf_op jit(solution)/shard_map/ppermute | solution.py:415
  6.4 20.7 %collective-permute-start.5 = (bf16[128,2048]{1,0:T(8,128)(2,1)S(1)}, bf16[128,2048]{1,0:T(8,128)(2,1)S(1)}, u32[]{:S(2)}, u32[]{:S(2)}) collective-permute-start(bf16[128,2048]{1,0:T(8,128)(2,1)S(1)} %bitcast.15), channel_id=1, source_target_pairs={{0,1},{1,0},{2,3},{3,2},{4,5},{5,4},{6,7},{7,6},{8,9},{9,8},{10,11... | collective-permute-start | bytes 1572872 | tf_op jit(solution)/shard_map/ppermute | solution.py:415
  6.8 4.0 %collective-permute-start = (bf16[2,2048]{1,0:T(2,128)(2,1)S(1)}, bf16[2,2048]{1,0:T(2,128)(2,1)S(1)}, u32[]{:S(2)}, u32[]{:S(2)}) collective-permute-start(bf16[2,2048]{1,0:T(2,128)(2,1)S(1)} %get-tuple-element.26), channel_id=1, source_target_pairs={{0,3},{1,2},{2,1},{3,0},{4,7},{5,6},{6,5},{7,4},{8,11},{9,10},{10,... | collective-permute-start | bytes 24584 | tf_op jit(solution)/shard_map/ppermute | solution.py:412
  9.4 3.7 %collective-permute-start.1 = (bf16[2,2048]{1,0:T(2,128)(2,1)S(1)}, bf16[2,2048]{1,0:T(2,128)(2,1)S(1)}, u32[]{:S(2)}, u32[]{:S(2)}) collective-permute-start(bf16[2,2048]{1,0:T(2,128)(2,1)S(1)} %get-tuple-element.27), channel_id=1, source_target_pairs={{0,2},{1,3},{2,0},{3,1},{4,6},{5,7},{6,4},{7,5},{8,10},{9,11},{10,... | collective-permute-start | bytes 24584 | tf_op jit(solution)/shard_map/ppermute | solution.py:412
  10.8 2.3 %collective-permute-start.2 = (bf16[2,2048]{1,0:T(2,128)(2,1)S(1)}, bf16[2,2048]{1,0:T(2,128)(2,1)S(1)}, u32[]{:S(2)}, u32[]{:S(2)}) collective-permute-start(bf16[2,2048]{1,0:T(2,128)(2,1)S(1)} %get-tuple-element.28), channel_id=1, source_target_pairs={{0,1},{1,0},{2,3},{3,2},{4,5},{5,4},{6,7},{7,6},{8,9},{9,8},{10,11... | collective-permute-start | bytes 24584 | tf_op jit(solution)/shard_map/ppermute | solution.py:412

commit v6 on v5

--- a/solution.py
+++ b/solution.py
@@ -191,7 +191,8 @@
         jnp.abs(jnp.sum(queries * grown, axis=1, keepdims=True)), jnp.exp(-stab)
     )
     named = routes[...].astype(F32)
-    lanes = lax.broadcasted_iota(jnp.int32, factors_out.shape, 1)
+    lane_width = -(-factors_out.shape[0] // 128) * 128
+    lanes = lax.broadcasted_iota(jnp.int32, (seq_rows, lane_width), 1)
     expert_of = lanes.astype(F32)
     share = jnp.zeros(lanes.shape, F32)
     for k in range(routes.shape[0]):
@@ -203,7 +204,9 @@
         return [array[portion * t : portion * (t + 1)] for t in range(c, tp_size, 2)]
 
     factors = jnp.where(lanes == ep_id, 1.0, share)
-    factors_out[...] = jnp.concatenate(side(factors, 0) + side(factors, 1), axis=0)
+    ordered = jnp.concatenate(side(factors, 0) + side(factors, 1), axis=0)
+    for e in range(factors_out.shape[0]):
+        factors_out[e] = jnp.broadcast_to(ordered[:, e : e + 1], factors_out.shape[1:])
     local = jnp.sum(jnp.where(lanes == ep_id, share, 0.0), axis=1, keepdims=True)
     local = jnp.where(
         tp_id & 1 == 0,
@@ -311,7 +314,8 @@
             value = returned[e * tp_size + c].astype(F32)
             for x in range(1, tp_size // 2):
                 value = value + returned[e * tp_size + 2 * x + c].astype(F32)
-            total = total + factors[rows, e : e + 1] * value
+            factor = jnp.concatenate([factors[e, rows, :]] * (value.shape[1] // 128), axis=1)
+            total = total + factor * value
         totals.append(total)
     pieces = [
         totals[t % 2][portion * (t // 2) : portion * (t // 2 + 1)] for t in range(tp_size)
@@ -375,14 +379,13 @@
         routes.T,
         route_weight.T,
     )
-    lane_width = -(-ep_size // 128) * 128
     peers = tp_size - 1
     results = pl.pallas_call(
         functools.partial(cell_kernel, tp_size=tp_size),
         out_shape=(
             *[shape((portion, width), BF16)] * peers,
             shape((portion, width), F32),
-            shape((seq_rows, lane_width), F32),
+            shape((ep_size, seq_rows, 128), F32),
             shape((ep_size * half, 128), F32),
             shape((ep_size * half, 128), F32),
             shape(normalizer.shape, F32),

time: 38.8 us -> 38.8 us (level)
  no operation moved by 1% of the time
where the time goes in v6:
time: 38.8 us; the launch traced here: 38.6 us
  blocking collectives  23.9 us (62%)
  Pallas kernels  5.97 us (15%)
  starting transfers between devices  3.74 us (10%)
  waiting for transfers between devices  3.58 us (9%)
  between operations  1.36 us (4%)
    all_to_all x1, blocking collectives, shards(): lax.all_to_all(outbound, BOTH, 0, 0, tiled=True, axis_index_groups=same_s...  13.8 us
    all_to_all x1, blocking collectives, shards(): returned = lax.all_to_all(blocks, BOTH, 0, 0, tiled=True)  10.2 us
    pallas_call x1, Pallas kernels, shards(): pl.pallas_call(functools.partial(cell_kernel, tp_size=tp_size), out_shape...  4.38 us
    ppermute x3, waiting for transfers between devices, shards(): lax.ppermute(sents[r - 1], 'tp', [(t, t ^ r) for t in range(tp_size)])  3.57 us
    ppermute x3, starting transfers between devices, shards(): lax.ppermute(sents[r - 1], 'tp', [(t, t ^ r) for t in range(tp_size)])  2.67 us
    ppermute x3, starting transfers between devices, shards(): mates = [lax.ppermute(weight, 'tp', swap) for weight in weights]  1.07 us
  transfers between devices with their start and end apart: 6, of which 2 were waited for; matrix products, arithmetic and copies ran while one was open for 0% of the time, Pallas kernels for 1%

profile of v6, /device:TPU:0, one launch (start us, length us, event | category | flops | bytes accessed | tf_op | source)
XLA Modules:
  0.0 38.6 jit_solution(14846524879144144796)
XLA Ops:
  1.3 0.0 copy-start
  1.3 0.0 copy-start.1
  1.3 0.0 copy-start.2
  1.3 0.0 copy-start.3
  1.3 4.4 %cell.1 = (bf16[2,2048]{1,0:T(2,128)(2,1)S(1)}, bf16[2,2048]{1,0:T(2,128)(2,1)S(1)}, bf16[2,2048]{1,0:T(2,128)(2,1)S(1)}, f32[2,2048]{1,0:T(2,128)S(1)}, f32[8,8...) custom-call(f32[1]{0:T(128)S(6)} %copy.23.bias, ...), custom_call_target="tpu_custom_call" | custom-call | tf_op jit(solution)/shard_map/cell/pallas_call | solution.py:383
  5.7 0.0 copy-done
  5.7 0.6 %collective-permute-start.3 = (bf16[2048,128]{1,0:T(8,128)(2,1)S(1)}, bf16[2048,128]{1,0:T(8,128)(2,1)S(1)}, u32[]{:S(2)}, u32[]{:S(2)}) collective-permute-start(bf16[2048,128]{1,0:T(8,128)(2,1)S(1)} %bitcast.11), channel_id=1, source_target_pairs={{0,1},{1,0},{2,3},{3,2},{4,5},{5,4},{6,7},{7,6},{8,9},{9,8},{10,11... | collective-permute-start | bytes 1572872 | tf_op jit(solution)/shard_map/ppermute | solution.py:418
  6.3 0.0 copy-done.1
  6.3 0.1 collective-permute-start.4
  6.4 0.0 copy-done.2
  6.4 0.4 %collective-permute-start.5 = (bf16[128,2048]{1,0:T(8,128)(2,1)S(1)}, bf16[128,2048]{1,0:T(8,128)(2,1)S(1)}, u32[]{:S(2)}, u32[]{:S(2)}) collective-permute-start(bf16[128,2048]{1,0:T(8,128)(2,1)S(1)} %bitcast.15), channel_id=1, source_target_pairs={{0,1},{1,0},{2,3},{3,2},{4,5},{5,4},{6,7},{7,6},{8,9},{9,8},{10,11... | collective-permute-start | bytes 1572872 | tf_op jit(solution)/shard_map/ppermute | solution.py:418
  6.8 2.6 %collective-permute-start = (bf16[2,2048]{1,0:T(2,128)(2,1)S(1)}, bf16[2,2048]{1,0:T(2,128)(2,1)S(1)}, u32[]{:S(2)}, u32[]{:S(2)}) collective-permute-start(bf16[2,2048]{1,0:T(2,128)(2,1)S(1)} %get-tuple-element.26), channel_id=1, source_target_pairs={{0,3},{1,2},{2,1},{3,0},{4,7},{5,6},{6,5},{7,4},{8,11},{9,10},{10,... | collective-permute-start | bytes 24584 | tf_op jit(solution)/shard_map/ppermute | solution.py:415
  9.4 0.0 collective-permute-start.1
  9.4 1.4 %collective-permute-done.rest_0_ = bf16[2,2048]{1,0:T(2,128)(2,1)S(1)} collective-permute-done((bf16[2,2048]{1,0:T(2,128)(2,1)S(1)}, bf16[2,2048]{1,0:T(2,128)(2,1)S(1)}, u32[]{:S(2)}, u32[]{:S(2)}) %collective-permute-start) | collective-permute-done | bytes 8224 | tf_op jit(solution)/shard_map/ppermute | solution.py:415
  10.8 0.1 collective-permute-start.2
  10.8 2.2 %collective-permute-done.1.rest_1_ = bf16[2,2048]{1,0:T(2,128)(2,1)S(1)} collective-permute-done((bf16[2,2048]{1,0:T(2,128)(2,1)S(1)}, bf16[2,2048]{1,0:T(2,128)(2,1)S(1)}, u32[]{:S(2)}, u32[]{:S(2)}) %collective-permute-start.1) | collective-permute-done | bytes 8224 | tf_op jit(solution)/shard_map/ppermute | solution.py:415
  13.0 0.0 collective-permute-done.2.rest_2_
  13.0 0.0 copy-done.3
  13.0 0.2 spread.1
  13.3 13.8 %all_to_all.10.arrived = bf16[16,2,2048]{2,1,0:T(2,128)(2,1)S(1)} all-to-all(bf16[16,2,2048]{2,1,0:T(2,128)(2,1)S(1)} %get-tuple-element.29), channel_id=1, replica_groups={{0,2,4,6,8,10,12,14,16,18,20,22,24,26,28,30},{1,3,5,7,9,11,13,15,17,19,..., dimensions={0} | all-to-all | bytes 262144 | tf_op jit(solution)/shard_map/all_to_all | solution.py:430
  27.0 0.0 collective-permute-done.3.gate_b
  27.0 0.0 collective-permute-done.4.up_b
  27.0 0.0 collective-permute-done.5.down_b
  27.1 0.7 %experts.1 = bf16[32,4,512]{2,1,0:T(4,128)(2,1)S(1)} custom-call(bf16[16,2,2048]{2,1,0:T(2,128)(2,1)S(1)} %all_to_all.10.arrived, f32[32,128]{1,0:T(8,128)S(1)} %get-tuple-element.30.row_factor, f32[32,128]{1,0:T(8,128)S(1)} %get-tuple-element.31.row_carry, f32[2,2048]{1,0:T(2,128)S(1)} %get-tuple-element.32.residual, bf16[2048,128]{1,0:T(8,128)(2,1)S(1)} %bitcast.12, ...), custom_call_target="tpu_custom_call" | custom-call | tf_op jit(solution)/shard_map/experts/pallas_call | solution.py:433
  27.8 10.2 %all_to_all.11.returned = bf16[32,4,512]{2,1,0:T(4,128)(2,1)S(1)} all-to-all(bf16[32,4,512]{2,1,0:T(4,128)(2,1)S(1)} %experts.1), channel_id=1, replica_groups=mesh['ep'=8,'tp'=4] {'ep','tp'}, dimensions={0} | all-to-all | bytes 262144 | tf_op jit(solution)/shard_map/all_to_all | solution.py:445
  37.9 0.6 %combine.1 = bf16[8,512]{1,0:T(8,128)(2,1)} custom-call(bf16[32,4,512]{2,1,0:T(4,128)(2,1)S(1)} %all_to_all.11.returned, f32[8,8,128]{2,1,0:T(8,128)S(1)} %get-tuple-element.36.factors), custom_call_target="tpu_custom_call" | custom-call | tf_op jit(solution)/shard_map/combine/pallas_call | solution.py:446
Async XLA Ops:
  1.3 4.4 %copy-start = (bf16[1,2048,128]{2,1,0:T(8,128)(2,1)S(1)}, bf16[1,2048,128]{2,1,0:T(8,128)(2,1)}, u32[]{:S(2)}) copy-start(bf16[1,2048,128]{2,1,0:T(8,128)(2,1)} %param.33) | copy-start | bytes 1572868
  1.3 5.0 %copy-start.1 = (bf16[1,2048,128]{2,1,0:T(8,128)(2,1)S(1)}, bf16[1,2048,128]{2,1,0:T(8,128)(2,1)}, u32[]{:S(2)}) copy-start(bf16[1,2048,128]{2,1,0:T(8,128)(2,1)} %param.34) | copy-start | bytes 1572868
  1.3 5.1 %copy-start.2 = (bf16[1,128,2048]{2,1,0:T(8,128)(2,1)S(1)}, bf16[1,128,2048]{2,1,0:T(8,128)(2,1)}, u32[]{:S(2)}) copy-start(bf16[1,128,2048]{2,1,0:T(8,128)(2,1)} %param.35) | copy-start | bytes 1572868
  1.3 11.7 %copy-start.3 = (f32[2048]{0:T(1024)S(1)}, f32[2048]{0:T(1024)}, u32[]{:S(2)}) copy-start(f32[2048]{0:T(1024)} %param.29) | copy-start | bytes 24580
  5.7 21.3 %collective-permute-start.3 = (bf16[2048,128]{1,0:T(8,128)(2,1)S(1)}, bf16[2048,128]{1,0:T(8,128)(2,1)S(1)}, u32[]{:S(2)}, u32[]{:S(2)}) collective-permute-start(bf16[2048,128]{1,0:T(8,128)(2,1)S(1)} %bitcast.11), channel_id=1, source_target_pairs={{0,1},{1,0},{2,3},{3,2},{4,5},{5,4},{6,7},{7,6},{8,9},{9,8},{10,11... | collective-permute-start | bytes 1572872 | tf_op jit(solution)/shard_map/ppermute | solution.py:418
  6.3 20.8 %collective-permute-start.4 = (bf16[2048,128]{1,0:T(8,128)(2,1)S(1)}, bf16[2048,128]{1,0:T(8,128)(2,1)S(1)}, u32[]{:S(2)}, u32[]{:S(2)}) collective-permute-start(bf16[2048,128]{1,0:T(8,128)(2,1)S(1)} %bitcast.13), channel_id=1, source_target_pairs={{0,1},{1,0},{2,3},{3,2},{4,5},{5,4},{6,7},{7,6},{8,9},{9,8},{10,11... | collective-permute-start | bytes 1572872 | tf_op jit(solution)/shard_map/ppermute | solution.py:418
  6.4 20.7 %collective-permute-start.5 = (bf16[128,2048]{1,0:T(8,128)(2,1)S(1)}, bf16[128,2048]{1,0:T(8,128)(2,1)S(1)}, u32[]{:S(2)}, u32[]{:S(2)}) collective-permute-start(bf16[128,2048]{1,0:T(8,128)(2,1)S(1)} %bitcast.15), channel_id=1, source_target_pairs={{0,1},{1,0},{2,3},{3,2},{4,5},{5,4},{6,7},{7,6},{8,9},{9,8},{10,11... | collective-permute-start | bytes 1572872 | tf_op jit(solution)/shard_map/ppermute | solution.py:418
  6.8 4.0 %collective-permute-start = (bf16[2,2048]{1,0:T(2,128)(2,1)S(1)}, bf16[2,2048]{1,0:T(2,128)(2,1)S(1)}, u32[]{:S(2)}, u32[]{:S(2)}) collective-permute-start(bf16[2,2048]{1,0:T(2,128)(2,1)S(1)} %get-tuple-element.26), channel_id=1, source_target_pairs={{0,3},{1,2},{2,1},{3,0},{4,7},{5,6},{6,5},{7,4},{8,11},{9,10},{10,... | collective-permute-start | bytes 24584 | tf_op jit(solution)/shard_map/ppermute | solution.py:415
  9.4 3.7 %collective-permute-start.1 = (bf16[2,2048]{1,0:T(2,128)(2,1)S(1)}, bf16[2,2048]{1,0:T(2,128)(2,1)S(1)}, u32[]{:S(2)}, u32[]{:S(2)}) collective-permute-start(bf16[2,2048]{1,0:T(2,128)(2,1)S(1)} %get-tuple-element.27), channel_id=1, source_target_pairs={{0,2},{1,3},{2,0},{3,1},{4,6},{5,7},{6,4},{7,5},{8,10},{9,11},{10,... | collective-permute-start | bytes 24584 | tf_op jit(solution)/shard_map/ppermute | solution.py:415
  10.8 2.3 %collective-permute-start.2 = (bf16[2,2048]{1,0:T(2,128)(2,1)S(1)}, bf16[2,2048]{1,0:T(2,128)(2,1)S(1)}, u32[]{:S(2)}, u32[]{:S(2)}) collective-permute-start(bf16[2,2048]{1,0:T(2,128)(2,1)S(1)} %get-tuple-element.28), channel_id=1, source_target_pairs={{0,1},{1,0},{2,3},{3,2},{4,5},{5,4},{6,7},{7,6},{8,9},{9,8},{10,11... | collective-permute-start | bytes 24584 | tf_op jit(solution)/shard_map/ppermute | solution.py:415
